TPU v7x, 32 devices: a whole 2x2x4 slice. The times are simulated.
32 devices in a mesh: grp: 2 (over y), sp: 8 (over z, core), tp: 2 (over x).
Axes of the slice: x: 2, y: 2, z: 4, core: 2. Of those that a mesh axis runs over, the one named last changes fastest.
Arguments:
- out_gate: bfloat16 [6144, 1024], P(('grp', 'sp'), 'tp'), parts along dimension 0, may hold values from -6 to 6
- in_gate: bfloat16 [6144, 1024], P(('grp', 'sp'), 'tp'), parts along dimension 0, may hold values from -6 to 6
- conv_input: bfloat16 [6144, 1024], P(('grp', 'sp'), 'tp'), parts along dimension 0, may hold values from -6 to 6
- doc_ids: int32 [6144], P(('grp', 'sp')), parts along dimension 0, may hold values from 0 to 3, never falling along the last dimension, each value on 1 to 1536 neighbouring positions
- residual: bfloat16 [6144, 2048], P(('grp', 'sp'), 'tp'), parts along dimension 0, may hold values from -6 to 6
- conv_taps: float32 [3, 1024], P(None, 'tp'), may hold values from -6 to 6
- mix_gain: float32 [1024], P('tp'), may hold values from 0.1 to 1.9
- out_weight: bfloat16 [1024, 2048], P('tp'), may hold values from -0.1875 to 0.1875
- ffn_gain: float32 [2048], P('tp'), may hold values from 0.1 to 1.9
- routing: int32 [6144, 2], P(('grp', 'sp')), parts along dimension 0, may hold values from 0 to 15, as said below
- route_weight: float32 [6144, 2], P(('grp', 'sp')), parts along dimension 0, may hold values from 0.2 to 1.2
- expert_gate: bfloat16 [16, 2048, 512], P('sp', None, 'tp'), may hold values from -0.125 to 0.125
- expert_up: bfloat16 [16, 2048, 512], P('sp', None, 'tp'), may hold values from -0.125 to 0.125
- expert_down: bfloat16 [16, 512, 2048], P('sp', None, 'tp'), may hold values from -0.25 to 0.25
- shared_gate: bfloat16 [2048, 512], P(None, 'tp'), may hold values from -0.125 to 0.125
- shared_up: bfloat16 [2048, 512], P(None, 'tp'), may hold values from -0.125 to 0.125
- shared_down: bfloat16 [512, 2048], P(None, 'tp'), may hold values from -0.25 to 0.25
Outputs:
- layer_out: bfloat16 [6144, 2048], P(('grp', 'sp'), 'tp'), parts along dimension 0
There are 2 independent parts, one for each index of `grp`. A program takes and returns all parts, laid end to end along the dimension named above; an argument that names none is the same for every part. Nothing has to cross between parts.
Inputs may be any that keep to these rules, and one draw needn't show every extreme that they name: `routing`: each row names 2 different experts. In each aligned block of 192 rows no expert is named by more than 48 rows, and some expert is named by exactly 48 rows. `doc_ids`: never falls along the sequence; a document holds at most 1536 positions.
All inputs are finite; a program needn't handle non-finite values.
Results may differ from a plain program's by a relative error of at most 0.017.
Values may be sent and summed in bfloat16 or wider, within the bound.
A program may use at most 64 MiB of HBM per device.

v0:
```python
import functools

import jax
import jax.numpy as jnp
from jax import lax
from jax.experimental import pallas as pl
from jax.experimental.pallas import tpu as pltpu
from jax.sharding import PartitionSpec as P

D_CONV = 1024
CONV_K = 3
TOPK = 2
EXP_DEV = 2


def from_behind(value, axis, steps):
    count = lax.axis_size(axis)
    first, last = (max(0, -steps), min(count, count - steps))
    return lax.ppermute(value, axis, [(source, source + steps) for source in range(first, last)])


def body(
    out_gate,
    in_gate,
    conv_input,
    doc_ids,
    residual,
    conv_taps,
    mix_gain,
    out_weight,
    ffn_gain,
    routing,
    route_weight,
    expert_gate,
    expert_up,
    expert_down,
    shared_gate,
    shared_up,
    shared_down,
):
    tokens = residual.shape[0]
    width = out_weight.shape[1]
    n_tp = lax.axis_size("tp")
    n_sp = lax.axis_size("sp")
    rows = tokens // n_tp
    experts = n_sp * EXP_DEV
    most = max(1, 2 * rows * TOPK // experts)
    slots = n_tp * most
    total = experts * slots
    cols = expert_down.shape[2]
    product = (in_gate.astype(jnp.float32) * conv_input.astype(jnp.float32)).astype(jnp.bfloat16)
    tail = (product[tokens - CONV_K + 1 :], doc_ids[tokens - CONV_K + 1 :].astype(jnp.bfloat16))
    prev_rows, prev_docs = from_behind((tail[0], tail[1]), "sp", 1)
    extended = jnp.concatenate([prev_rows, product], axis=0).astype(jnp.float32)
    ext_docs = jnp.concatenate([prev_docs.astype(jnp.int32), doc_ids])
    mixed = jnp.zeros(product.shape, jnp.float32)
    for k in range(CONV_K):
        keep = (ext_docs[k : k + tokens] == doc_ids)[:, None]
        mixed = mixed + jnp.where(keep, conv_taps[k] * extended[k : k + tokens], jnp.float32(0.0))
    conv_out = out_gate.astype(jnp.float32) * mixed
    squares = lax.psum(jnp.sum(conv_out * conv_out, axis=1), "tp")
    normed = (conv_out * lax.rsqrt(squares / D_CONV + 1e-06)[:, None] * mix_gain).astype(
        jnp.bfloat16
    )
    partial_value = jnp.dot(normed, out_weight, preferred_element_type=jnp.float32)
    proj = lax.psum_scatter(
        partial_value.astype(jnp.bfloat16), "tp", scatter_dimension=1, tiled=True
    ).astype(jnp.float32)
    stream = (residual.astype(jnp.float32) + proj).astype(jnp.bfloat16)
    stream32 = stream.astype(jnp.float32)
    stream_sq = lax.psum(jnp.sum(stream32 * stream32, axis=1), "tp")
    normal_cols = (stream32 * lax.rsqrt(stream_sq / width + 1e-06)[:, None] * ffn_gain).astype(
        jnp.bfloat16
    )
    flat_expert = routing.reshape(-1)
    onehot = (flat_expert[:, None] == jnp.arange(experts, dtype=jnp.int32)[None, :]).astype(
        jnp.int32
    )
    blocked = onehot.reshape(n_tp, rows * TOPK, experts)
    earlier = jnp.cumsum(blocked, axis=1) - blocked
    position = jnp.sum(earlier * blocked, axis=2).reshape(-1)
    entry = jnp.arange(tokens * TOPK, dtype=jnp.int32)
    slot = flat_expert * slots + entry // (rows * TOPK) * most + position
    table = jnp.full((total,), tokens, jnp.int32).at[slot].set(entry // TOPK)
    block_rows = lax.all_to_all(normal_cols, "tp", split_axis=0, concat_axis=1, tiled=True)
    mine = lax.dynamic_index_in_dim(
        table.reshape(n_sp, EXP_DEV, n_tp, most), lax.axis_index("tp"), 2, False
    )
    local = jnp.where(mine >= tokens, rows, mine - lax.axis_index("tp") * rows)
    padded_block = jnp.concatenate([block_rows, jnp.zeros((1, width), jnp.bfloat16)], axis=0)
    got = lax.all_to_all(padded_block[local], "sp", split_axis=0, concat_axis=0, tiled=True)
    arrived, whole = (
        lax.all_gather(got, "tp", axis=2, tiled=True),
        lax.all_gather(block_rows.reshape(1, 1, rows, width), "tp", axis=2, tiled=True),
    )
    normal = whole.reshape(tokens, width)
    gate = jnp.einsum("nesd,edh->nesh", arrived, expert_gate, preferred_element_type=jnp.float32)
    upper = jnp.einsum("nesd,edh->nesh", arrived, expert_up, preferred_element_type=jnp.float32)
    hidden = (jax.nn.silu(gate) * upper).astype(jnp.bfloat16)
    hidden_flat = hidden.reshape(n_sp * EXP_DEV * slots, hidden.shape[3])
    shared_hid = (
        jax.nn.silu(jnp.dot(normal, shared_gate, preferred_element_type=jnp.float32))
        * jnp.dot(normal, shared_up, preferred_element_type=jnp.float32)
    ).astype(jnp.bfloat16)
    expert_piece = lax.all_gather(hidden_flat, "tp", axis=1, tiled=True)
    shared_piece = lax.all_gather(shared_hid, "tp", axis=1, tiled=True)
    count = expert_piece.shape[1]
    expert_part = jnp.einsum(
        "nesh,ehd->nesd",
        expert_piece.reshape(n_sp, EXP_DEV, slots, count),
        expert_down,
        preferred_element_type=jnp.float32,
    )
    shared_part = jnp.dot(shared_piece, shared_down, preferred_element_type=jnp.float32)
    returned = lax.all_to_all(
        expert_part.astype(jnp.bfloat16), "sp", split_axis=0, concat_axis=0, tiled=True
    )
    picked = (
        returned.reshape(total, cols)[slot].astype(jnp.float32) * route_weight.reshape(-1)[:, None]
    )
    routed = jnp.sum(picked.reshape(tokens, TOPK, cols), axis=1)
    return (stream32 + shared_part + routed).astype(jnp.bfloat16)


MESH = pl.DeviceIdType.MESH
F32 = jnp.float32
BF16 = jnp.bfloat16


def silu_mul(gate, upper):
    return (gate / (1.0 + jnp.exp(-gate)) * upper).astype(BF16)


def mm(a, b):
    return jnp.dot(a, b, preferred_element_type=F32)


def moe_kernel(
    n_z,
    most,
    own_ref,
    own_meta,
    gain_ref,
    wg_hbm,
    wu_hbm,
    wd_hbm,
    sg_hbm,
    su_hbm,
    sd_hbm,
    out_ref,
    wg,
    wu,
    wd,
    sg,
    su,
    sd,
    blk,
    meta,
    xs,
    hid,
    shid,
    ys,
    acc,
    outgo,
    sib,
    back,
    fin,
    send_sem,
    recv_sem,
    hid_send,
    hid_recv,
    sh_sem,
    sib_send,
    sib_recv,
    back_send,
    back_recv,
    load_sem,
):
    loads = [
        pltpu.make_async_copy(src, dst, load_sem.at[n])
        for n, (src, dst) in enumerate(
            (
                (wg_hbm, wg),
                (wu_hbm, wu),
                (sg_hbm, sg),
                (su_hbm, su),
                (wd_hbm, wd),
                (sd_hbm, sd),
            )
        )
    ]
    for load in loads:
        load.start()
    s = lax.axis_index("sp")
    t = lax.axis_index("tp")
    z = s // 2
    c = s % 2
    rows, width = own_ref.shape
    cols = out_ref.shape[2]
    half = wg.shape[2]
    per, piece = acc.shape[1] // 2, acc.shape[2]
    lo = z > 0
    hi = z < n_z - 1
    up, down = {"sp": s + 2}, {"sp": s - 2}
    other, peer = {"sp": s + 1 - 2 * c}, {"tp": 1 - t}
    targets = (up, down, peer, other)

    def slot(zq, cq, tq):
        return (zq * 2 + cq) * 2 + tq

    def zone(i):
        return z + (1 - 2 * (i % 2)) * ((i + 1) // 2)

    def valid(i):
        zq = zone(i)
        return (i >= 0) & (i <= 2 * n_z - 2) & (zq >= 0) & (zq < n_z)

    def remote(src, dst, ssem, rsem, dev):
        return pltpu.make_async_remote_copy(
            src_ref=src,
            dst_ref=dst,
            send_sem=ssem,
            recv_sem=rsem,
            device_id=dev,
            device_id_type=MESH,
        )

    def block(b, way, own=False):
        return (
            remote(
                own_ref if own else blk.at[b],
                blk.at[b],
                send_sem.at[way, b, 0],
                recv_sem.at[b, 0],
                targets[way],
            ),
            remote(
                own_meta if own else meta.at[b],
                meta.at[b],
                send_sem.at[way, b, 1],
                recv_sem.at[b, 1],
                targets[way],
            ),
        )

    def start(b, way, own=False):
        for copy in block(b, way, own):
            copy.start()

    def arrived(b):
        for copy in block(b, 2):
            copy.wait_recv()

    def hid_copy(zq):
        return remote(hid.at[t, zq], hid.at[t, zq], hid_send.at[zq], hid_recv.at[zq], peer)

    def sh_copy():
        return remote(shid.at[t], shid.at[t], sh_sem.at[0], sh_sem.at[1], peer)

    def sib_copy(zq):
        return remote(outgo.at[zq], sib.at[zq], sib_send.at[zq], sib_recv.at[zq], other)

    def back_copy(zq, q, to, dev):
        return remote(
            acc.at[zq, q],
            back.at[to, q],
            back_send.at[zq, q],
            back_recv.at[to, q],
            dev,
        )

    def pass_on(zq, q):
        @pl.when(zq > z)
        def _():
            back_copy(zq, q, zq, up).start()

        @pl.when(zq < z - 1)
        def _():
            back_copy(zq, q, zq, down).start()

        @pl.when(zq == z - 1)
        def _():
            back_copy(zq, q, n_z, down).start()

    barrier = pltpu.get_barrier_semaphore()
    for way, there in ((0, hi), (1, lo)):

        @pl.when(there)
        def _():
            pl.semaphore_signal(barrier, inc=1, device_id=targets[way], device_id_type=MESH)

    for way in (2, 3):
        pl.semaphore_signal(barrier, inc=1, device_id=targets[way], device_id_type=MESH)
    pl.semaphore_wait(barrier, 2 + lo.astype(jnp.int32) + hi.astype(jnp.int32))

    mine = slot(z, c, t)

    @pl.when(hi)
    def _():
        start(mine, 0, True)

    @pl.when(lo)
    def _():
        start(mine, 1, True)

    start(mine, 2, True)
    start(mine, 3, True)
    blk[mine] = own_ref[...]
    meta[mine] = own_meta[...]

    def picks(b):
        pair = meta[b, z][:, :rows]
        info = jnp.where(c == 0, pair[: 2 * EXP_DEV], pair[2 * EXP_DEV :])
        place = lax.broadcasted_iota(jnp.int32, (most, rows), 0).astype(F32)
        return info, [(info[e : e + 1] == place).astype(F32) for e in range(EXP_DEV)]

    def normalise(value):
        ms = jnp.mean(value * value, axis=1, keepdims=True)
        return (value * lax.rsqrt(ms + 1e-06) * gain_ref[...]).astype(BF16)

    def group(j):
        return [(p, tq, c + p - 2 * c * p) for p in range(2) for tq in range(2)]

    def hidden(zq):
        for j, (p, tq, cq) in enumerate(group(zq)):
            b = slot(zq, cq, tq)
            _, chosen = picks(b)
            sel = jnp.concatenate(chosen, axis=0).astype(BF16)
            got = normalise(mm(sel, blk[b]))
            for e in range(EXP_DEV):
                xs[e, j * most : (j + 1) * most, :] = got[e * most : (e + 1) * most]
        for e in range(EXP_DEV):
            hid[t, zq, e] = silu_mul(mm(xs[e], wg[e]), mm(xs[e], wu[e]))

    def shared():
        for tq in range(2):
            whole = normalise(blk[slot(z, c, tq)].astype(F32))
            shid[t, tq] = silu_mul(mm(whole, sg[...]), mm(whole, su[...]))

    def results(zq):
        hid_copy(zq).wait_recv()
        for e in range(EXP_DEV):
            ys[e] = (
                mm(hid[0, zq, e], wd[e, :half, :]) + mm(hid[1, zq, e], wd[e, half:, :])
            ).astype(BF16)
        for j, (p, tq, cq) in enumerate(group(zq)):
            info, chosen = picks(slot(zq, cq, tq))
            parts = []
            for e in range(EXP_DEV):
                weight = jnp.sum(
                    chosen[e] * info[EXP_DEV + e : EXP_DEV + e + 1], axis=1, keepdims=True
                )
                part = ys[e, j * most : (j + 1) * most, :].astype(F32)
                parts.append((part * weight).astype(BF16))
            sel = jnp.concatenate(chosen, axis=0).astype(BF16)
            spread = lax.dot_general(
                sel,
                jnp.concatenate(parts, axis=0),
                (((0,), (0,)), ((), ())),
                preferred_element_type=F32,
            ).astype(BF16)
            into = acc if p == 0 else outgo
            for h in range(per):
                into[zq, tq * per + h] = spread[h * piece : (h + 1) * piece]
        sib_copy(zq).start()

    def is_end(zq):
        return ((zq > z) & jnp.logical_not(lo)) | ((zq < z) & jnp.logical_not(hi))

    for load in loads[:2]:
        load.wait()

    @pl.loop(1, 2 * n_z + 3)
    def _(i):
        @pl.when(valid(i))
        def _():
            zq = zone(i)
            b = slot(zq, c, t)
            arrived(b)

            @pl.when(hi & (zq < z))
            def _():
                start(b, 0)

            @pl.when(lo & (zq > z))
            def _():
                start(b, 1)

            start(b, 2)
            start(b, 3)

        @pl.when(valid(i - 4))
        def _():
            zq = zone(i - 4)
            results(zq)

            @pl.when(is_end(zq))
            def _():
                sib_copy(zq).wait_recv()
                for q in range(2 * per):
                    acc[zq, q] = (acc[zq, q].astype(F32) + sib[zq, q].astype(F32)).astype(BF16)
                    pass_on(zq, q)

        @pl.when(valid(i - 2))
        def _():
            zq = zone(i - 2)
            b = slot(zq, c, 1 - t)
            arrived(b)
            start(b, 3)
            arrived(slot(zq, 1 - c, t))
            arrived(slot(zq, 1 - c, 1 - t))
            hidden(zq)
            hid_copy(zq).start()

        @pl.when(i == 3)
        def _():
            for load in loads[2:]:
                load.wait()
            shared()

        @pl.when(i == 2 * n_z)
        def _():
            sh_copy().start()


    above = n_z - 1 - z
    up_first = (above >= z).astype(jnp.int32)

    def through(k):
        in_up = (k < above).astype(jnp.int32)
        in_down = (k < z).astype(jnp.int32)
        rise = in_up * (z + 1 + k) + (1 - in_up) * (z - 1 - (k - above))
        fall = in_down * (z - 1 - k) + (1 - in_down) * (z + 1 + (k - z))
        return up_first * rise + (1 - up_first) * fall

    def relay(k, q):
        zq = through(k)

        @pl.when(jnp.logical_not(is_end(zq)))
        def _():
            if q == 0:
                sib_copy(zq).wait_recv()
            back_copy(zq, q, zq, up).wait_recv()
            acc[zq, q] = (
                acc[zq, q].astype(F32) + sib[zq, q].astype(F32) + back[zq, q].astype(F32)
            ).astype(BF16)
            pass_on(zq, q)

    for q in range(2 * per):
        relay(0, q)
    for q in range(2 * per):
        for k in range(1, n_z - 1):
            relay(k, q)

    sib_copy(z).wait_recv()
    sh_copy().wait_recv()
    for tq in range(2):
        stream = blk[slot(z, c, tq), :, pl.ds(pl.multiple_of(t * cols, cols), cols)]
        base = (
            stream.astype(F32)
            + mm(shid[0, tq], sd[:half, :])
            + mm(shid[1, tq], sd[half:, :])
        )
        for h in range(per):
            q = tq * per + h
            fin[q] = (
                base[h * piece : (h + 1) * piece]
                + acc[z, q].astype(F32)
                + sib[z, q].astype(F32)
            )
    for q in range(2 * per):

        @pl.when(lo)
        def _():
            back_copy(z, q, z, up).wait_recv()
            fin[q] = fin[q] + back[z, q].astype(F32)

        @pl.when(hi)
        def _():
            back_copy(z, q, n_z, up).wait_recv()
            fin[q] = fin[q] + back[n_z, q].astype(F32)

        tq, h = divmod(q, per)
        out_ref[tq, h * piece : (h + 1) * piece, :] = fin[q].astype(BF16)

    @pl.loop(0, n_z)
    def _(zq):
        b = slot(zq, c, t)

        @pl.when(hi & (zq <= z))
        def _():
            for copy in block(b, 0):
                copy.wait_send()

        @pl.when(lo & (zq >= z))
        def _():
            for copy in block(b, 1):
                copy.wait_send()

        for copy in block(b, 2) + block(b, 3) + block(slot(zq, c, 1 - t), 3):
            copy.wait_send()
        hid_copy(zq).wait_send()
        sib_copy(zq).wait_send()

        @pl.when(zq != z)
        def _():
            for q in range(2 * per):
                back_copy(zq, q, zq, up).wait_send()

    sh_copy().wait_send()


def fast(
    out_gate,
    in_gate,
    conv_input,
    doc_ids,
    residual,
    conv_taps,
    mix_gain,
    out_weight,
    ffn_gain,
    routing,
    route_weight,
    expert_gate,
    expert_up,
    expert_down,
    shared_gate,
    shared_up,
    shared_down,
):
    tokens, cols = residual.shape
    width = out_weight.shape[1]
    n_tp, n_sp = lax.axis_size("tp"), lax.axis_size("sp")
    n_z = n_sp // 2
    rows = tokens // n_tp
    experts = n_sp * EXP_DEV
    most = max(1, 2 * rows * TOPK // experts)
    t = lax.axis_index("tp")
    swap = [(0, 1), (1, 0)]

    def cut(value, who):
        return lax.dynamic_slice_in_dim(value, who * rows, rows, 0)

    res_other = lax.ppermute(cut(residual, 1 - t), "tp", swap)
    product = (in_gate.astype(F32) * conv_input.astype(F32)).astype(BF16)
    prev_rows, prev_docs = from_behind(
        (product[tokens - CONV_K + 1 :], doc_ids[tokens - CONV_K + 1 :].astype(BF16)), "sp", 1
    )
    extended = jnp.concatenate([prev_rows, product], axis=0).astype(F32)
    ext_docs = jnp.concatenate([prev_docs.astype(jnp.int32), doc_ids])
    mixed = jnp.zeros(product.shape, F32)
    for k in range(CONV_K):
        keep = (ext_docs[k : k + tokens] == doc_ids)[:, None]
        mixed = mixed + jnp.where(keep, conv_taps[k] * extended[k : k + tokens], F32(0.0))
    conv_out = out_gate.astype(F32) * mixed
    sums = jnp.sum(conv_out * conv_out, axis=1)
    sums_other = lax.ppermute(sums, "tp", swap)
    gain_other = lax.ppermute(ffn_gain, "tp", swap)
    squares = sums + sums_other
    first = t == 0
    gain = jnp.concatenate(
        [jnp.where(first, ffn_gain, gain_other), jnp.where(first, gain_other, ffn_gain)]
    )
    normed = (conv_out * lax.rsqrt(squares / D_CONV + 1e-06)[:, None] * mix_gain).astype(BF16)
    given = mm(cut(normed, 1 - t), out_weight).astype(BF16)
    taken = lax.ppermute(given, "tp", swap)
    kept = lax.optimization_barrier(mm(cut(normed, t), out_weight).astype(BF16))
    res_mine = cut(residual, t)
    res = jnp.concatenate(
        [jnp.where(first, res_mine, res_other), jnp.where(first, res_other, res_mine)], axis=1
    )
    stream = (res.astype(F32) + (kept.astype(F32) + taken.astype(F32))).astype(BF16)

    names = cut(routing, t)
    weights = cut(route_weight, t)
    hot = names[:, :, None] == jnp.arange(experts, dtype=jnp.int32)
    named = jnp.any(hot, axis=1)
    placed = jnp.sum(jnp.where(hot, weights[:, :, None], F32(0.0)), axis=1)
    before = jnp.arange(rows)[:, None] > jnp.arange(rows)[None, :]
    earlier = mm(before.astype(BF16), named.astype(BF16))
    position = jnp.where(named, earlier, F32(-1.0))
    info = jnp.stack([position, placed], axis=0).reshape(2, rows, n_sp, EXP_DEV)
    info = info.transpose(2, 0, 3, 1).reshape(n_z, 4 * EXP_DEV, rows)
    pad = -rows % 128
    info = jnp.pad(info, ((0, 0), (0, 0), (0, pad)), constant_values=-1.0)

    per = 2
    piece = rows // per
    blocks = n_sp * n_tp
    half = expert_gate.shape[2]
    vm = pl.BlockSpec(memory_space=pltpu.VMEM)
    dma = pltpu.SemaphoreType.DMA
    out = pl.pallas_call(
        functools.partial(moe_kernel, n_z, most),
        out_shape=jax.ShapeDtypeStruct((n_tp, rows, cols), BF16),
        in_specs=[vm] * 3 + [pl.BlockSpec(memory_space=pl.ANY)] * 6,
        out_specs=vm,
        scratch_shapes=[
            pltpu.VMEM(expert_gate.shape, BF16),
            pltpu.VMEM(expert_up.shape, BF16),
            pltpu.VMEM(expert_down.shape, BF16),
            pltpu.VMEM(shared_gate.shape, BF16),
            pltpu.VMEM(shared_up.shape, BF16),
            pltpu.VMEM(shared_down.shape, BF16),
            pltpu.VMEM((blocks, rows, width), BF16),
            pltpu.VMEM((blocks,) + info.shape, F32),
            pltpu.VMEM((EXP_DEV, 4 * most, width), BF16),
            pltpu.VMEM((2, n_z, EXP_DEV, 4 * most, half), BF16),
            pltpu.VMEM((2, 2, rows, half), BF16),
            pltpu.VMEM((EXP_DEV, 4 * most, cols), BF16),
            pltpu.VMEM((n_z, 2 * per, piece, cols), BF16),
            pltpu.VMEM((n_z, 2 * per, piece, cols), BF16),
            pltpu.VMEM((n_z, 2 * per, piece, cols), BF16),
            pltpu.VMEM((n_z + 1, 2 * per, piece, cols), BF16),
            pltpu.VMEM((2 * per, piece, cols), F32),
            dma((4, blocks, 2)),
            dma((blocks, 2)),
            dma((n_z,)),
            dma((n_z,)),
            dma((2,)),
            dma((n_z,)),
            dma((n_z,)),
            dma((n_z, 2 * per)),
            dma((n_z + 1, 2 * per)),
            dma((6,)),
        ],
        compiler_params=pltpu.CompilerParams(
            collective_id=0, has_side_effects=True, vmem_limit_bytes=64 * 1024 * 1024 - 65536
        ),
    )(
        stream,
        info,
        gain[None, :],
        expert_gate,
        expert_up,
        expert_down,
        shared_gate,
        shared_up,
        shared_down,
    )
    return out.reshape(tokens, cols)


def fits(mesh):
    return mesh.shape["tp"] == 2 and mesh.shape["sp"] in (4, 6, 8)


def solution(mesh):
    return jax.shard_map(
        fast if fits(mesh) else body,
        mesh=mesh,
        in_specs=(
            P(("grp", "sp"), "tp"),
            P(("grp", "sp"), "tp"),
            P(("grp", "sp"), "tp"),
            P(("grp", "sp")),
            P(("grp", "sp"), "tp"),
            P(None, "tp"),
            P("tp"),
            P("tp", None),
            P("tp"),
            P(("grp", "sp"), None),
            P(("grp", "sp"), None),
            P("sp", None, "tp"),
            P("sp", None, "tp"),
            P("sp", None, "tp"),
            P(None, "tp"),
            P(None, "tp"),
            P(None, "tp"),
        ),
        out_specs=P(("grp", "sp"), "tp"),
        check_vma=False,
    )
```

profile of v0, /device:TPU:0, one launch (start us, length us, event | category | flops | bytes accessed | tf_op | source)
XLA Modules:
  0.0 190.8 jit_solution(10625317994958233755)
XLA Ops:
  0.0 1.2 multiply_convert_fusion.1
  1.2 2.4 %collective-permute-start.2 = (bf16[2,512]{1,0:T(2,128)(2,1)S(1)}, bf16[2,512]{1,0:T(2,128)(2,1)S(1)}, u32[]{:S(2)}, u32[]{:S(2)}) collective-permute-start(bf16[2,512]{1,0:T(2,128)(2,1)S(1)} %slice.41), channel_id=1, source_target_pairs={{0,2},{2,4},{4,6},{6,8},{8,10},{10,12},{12,14},{1,3},{3,5},{5,7},{... | collective-permute-start | bytes 6152 | tf_op jit(solution)/shard_map/ppermute | solution.py:19
  3.6 0.7 convert.3
  4.4 4.6 %collective-permute-start.1 = (bf16[2]{0:T(256)(128)(2,1)S(1)}, bf16[2]{0:T(256)(128)(2,1)S(1)}, u32[]{:S(2)}, u32[]{:S(2)}) collective-permute-start(bf16[2]{0:T(256)(128)(2,1)S(1)} %slice.31), channel_id=1, source_target_pairs={{0,2},{2,4},{4,6},{6,8},{8,10},{10,12},{12,14},{1,3},{3,5},{5,7},{... | collective-permute-start | bytes 20 | tf_op jit(solution)/shard_map/ppermute | solution.py:19
  9.0 1.8 constant_dynamic-slice_fusion.2
  10.8 1.5 collective-permute-start
  12.3 0.5 collective-permute-start.5
  12.8 0.8 fusion.11
  13.6 0.8 constant_dynamic-slice_fusion.1
  14.4 0.8 constant_dynamic-slice_fusion
  15.2 0.1 convolution_select_fusion
  15.7 1.7 multiply_reduce_fusion
  17.4 1.5 collective-permute-start.3
  19.0 0.6 pad.4.own_meta
  19.6 2.6 %collective-permute-done.3 = f32[384]{0:T(512)S(1)} collective-permute-done((f32[384]{0:T(512)S(1)}, f32[384]{0:T(512)S(1)}, u32[]{:S(2)}, u32[]{:S(2)}) %collective-permute-start.3) | collective-permute-done | bytes 1568 | tf_op jit(solution)/shard_map/ppermute | solution.py:558
  22.3 0.6 convolution_convert_fusion
  22.9 1.6 collective-permute-start.4
  24.5 0.6 convolution_convert_fusion.1
  25.1 0.6 pad_maximum_fusion
  25.7 0.2 broadcast_select_fusion.1
  25.9 15.7 %collective-permute-done.4 = bf16[192,2048]{1,0:T(8,128)(2,1)S(1)} collective-permute-done((bf16[192,2048]{1,0:T(8,128)(2,1)S(1)}, bf16[192,2048]{1,0:T(8,128)(2,1)S(1)}, u32[]{:S(2)}, u32[]{:S(2)}) %collective-permute-start.4) | collective-permute-done | bytes 786464 | tf_op jit(solution)/shard_map/ppermute | solution.py:567
  41.6 1.3 add_convert_fusion.own_ref
  42.9 145.9 %shard_map.163 = bf16[2,192,1024]{2,1,0:T(8,128)(2,1)} custom-call(bf16[192,2048]{1,0:T(8,128)(2,1)} %add_convert_fusion.own_ref, f32[4,8,256]{2,1,0:T(8,128)} %pad.4.own_meta, f32[1,2048]{1,0:T(1,128)} %bitcast.19, bf16[2,2048,256]{2,1,0:T(8,128)(2,1)} %wg_hbm.1, bf16[2,2048,256]{2,1,0:T(8,128)(2,1)} %wu_hbm.1, bf16[2,512,1024]{2,1,0:T(8,128)(2,1)} %wd_hbm.1, ...), custom_call_target="tpu_custom_call" | custom-call | tf_op jit(solution)/shard_map/pallas_call | solution.py:594
  188.7 2.1 %copy.24 = bf16[384,1024]{1,0:T(8,128)(2,1)} copy(bf16[384,1024]{1,0:T(8,128)(2,1)} %bitcast.16) | data formatting | bytes 1572864
  (29 shorter events, 0.6 us)
Async XLA Ops:
  0.0 15.4 %copy-start.2 = (s32[384]{0:T(512)S(1)}, s32[384]{0:T(512)}, u32[]{:S(2)}) copy-start(s32[384]{0:T(512)} %param.20) | copy-start | bytes 4612
  1.2 14.3 %collective-permute-start.2 = (bf16[2,512]{1,0:T(2,128)(2,1)S(1)}, bf16[2,512]{1,0:T(2,128)(2,1)S(1)}, u32[]{:S(2)}, u32[]{:S(2)}) collective-permute-start(bf16[2,512]{1,0:T(2,128)(2,1)S(1)} %slice.41), channel_id=1, source_target_pairs={{0,2},{2,4},{4,6},{6,8},{8,10},{10,12},{12,14},{1,3},{3,5},{5,7},{... | collective-permute-start | bytes 6152 | tf_op jit(solution)/shard_map/ppermute | solution.py:19
  4.4 11.0 %collective-permute-start.1 = (bf16[2]{0:T(256)(128)(2,1)S(1)}, bf16[2]{0:T(256)(128)(2,1)S(1)}, u32[]{:S(2)}, u32[]{:S(2)}) collective-permute-start(bf16[2]{0:T(256)(128)(2,1)S(1)} %slice.31), channel_id=1, source_target_pairs={{0,2},{2,4},{4,6},{6,8},{8,10},{10,12},{12,14},{1,3},{3,5},{5,7},{... | collective-permute-start | bytes 20 | tf_op jit(solution)/shard_map/ppermute | solution.py:19
  10.8 14.9 %collective-permute-start = (bf16[192,1024]{1,0:T(8,128)(2,1)}, bf16[192,1024]{1,0:T(8,128)(2,1)S(1)}, u32[]{:S(2)}, u32[]{:S(2)}) collective-permute-start(bf16[192,1024]{1,0:T(8,128)(2,1)} %constant_dynamic-slice_fusion.2), channel_id=1, source_target_pairs={{0,1},{1,0},{2,3},{3,2},{4,5},{5,4},{6,7},{7,6},{8,9},{9,8},{10,11... | collective-permute-start | bytes 1179656 | tf_op jit(solution)/shard_map/ppermute | solution.py:545
  12.3 12.8 %collective-permute-start.5 = (f32[1024]{0:T(1024)}, f32[1024]{0:T(1024)S(1)}, u32[]{:S(2)}, u32[]{:S(2)}) collective-permute-start(f32[1024]{0:T(1024)} %param.25), channel_id=1, source_target_pairs={{0,1},{1,0},{2,3},{3,2},{4,5},{5,4},{6,7},{7,6},{8,9},{9,8},{10,11... | collective-permute-start | bytes 12296 | tf_op jit(solution)/shard_map/ppermute | solution.py:559
  15.7 6.5 %copy-start.4 = (f32[512]{0:T(512)S(1)}, f32[512]{0:T(512)}, u32[]{:S(2)}) copy-start(f32[512]{0:T(512)} %param.23) | copy-start | bytes 6148
  15.7 6.6 %copy-start = (bf16[512,2048]{1,0:T(8,128)(2,1)S(1)}, bf16[512,2048]{1,0:T(8,128)(2,1)}, u32[]{:S(2)}) copy-start(bf16[512,2048]{1,0:T(8,128)(2,1)} %param.24) | copy-start | bytes 6291460
  17.4 4.8 %collective-permute-start.3 = (f32[384]{0:T(512)S(1)}, f32[384]{0:T(512)S(1)}, u32[]{:S(2)}, u32[]{:S(2)}) collective-permute-start(f32[384]{0:T(512)S(1)} %get-tuple-element.5), channel_id=1, source_target_pairs={{0,1},{1,0},{2,3},{3,2},{4,5},{5,4},{6,7},{7,6},{8,9},{9,8},{10,11... | collective-permute-start | bytes 4616 | tf_op jit(solution)/shard_map/ppermute | solution.py:558
  22.9 2.2 %copy-start.3 = (f32[1024]{0:T(1024)S(1)}, f32[1024]{0:T(1024)}, u32[]{:S(2)}) copy-start(f32[1024]{0:T(1024)} %param.25) | copy-start | bytes 12292
  22.9 2.8 %copy-start.1 = (bf16[384,1024]{1,0:T(8,128)(2,1)S(1)}, bf16[384,1024]{1,0:T(8,128)(2,1)}, u32[]{:S(2)}) copy-start(bf16[384,1024]{1,0:T(8,128)(2,1)} %param.21) | copy-start | bytes 2359300
  22.9 18.7 %collective-permute-start.4 = (bf16[192,2048]{1,0:T(8,128)(2,1)S(1)}, bf16[192,2048]{1,0:T(8,128)(2,1)S(1)}, u32[]{:S(2)}, u32[]{:S(2)}) collective-permute-start(bf16[192,2048]{1,0:T(8,128)(2,1)S(1)} %convolution_convert_fusion), channel_id=1, source_target_pairs={{0,1},{1,0},{2,3},{3,2},{4,5},{5,4},{6,7},{7,6},{8,9},{9,8},{10,11... | collective-permute-start | bytes 2359304 | tf_op jit(solution)/shard_map/ppermute | solution.py:567
where the time goes:
time: 192 us; the launch traced here: 191 us
  Pallas kernels  146 us (76%)
  waiting for transfers between devices  18.3 us (10%)
  starting transfers between devices  12.1 us (6%)
  local copies, waits for them, and re-layouts  6.96 us (4%)
  other arithmetic  6.1 us (3%)
    pallas_call x1, Pallas kernels, fast(): pl.pallas_call(functools.partial(moe_kernel, n_z, most), out_shape=jax.Sh...  146 us
    ppermute x1, waiting for transfers between devices, fast(): taken = lax.ppermute(given, 'tp', swap)  15.7 us
    ppermute x2, starting transfers between devices, from_behind(): lax.ppermute(value, axis, [(source, source + steps) for source in range(f...  6.97 us
  transfers between devices with their start and end apart: 6, of which 2 were waited for; matrix products, arithmetic and copies ran while one was open for 5% of the time, Pallas kernels for 0%

commit v1 on v0

v1 whole, which is shorter than its diff:
```python
import functools

import jax
import jax.numpy as jnp
from jax import lax
from jax.experimental import pallas as pl
from jax.experimental.pallas import tpu as pltpu
from jax.sharding import PartitionSpec as P

D_CONV = 1024
CONV_K = 3
TOPK = 2
EXP_DEV = 2


def from_behind(value, axis, steps):
    count = lax.axis_size(axis)
    first, last = (max(0, -steps), min(count, count - steps))
    return lax.ppermute(value, axis, [(source, source + steps) for source in range(first, last)])


def body(
    out_gate,
    in_gate,
    conv_input,
    doc_ids,
    residual,
    conv_taps,
    mix_gain,
    out_weight,
    ffn_gain,
    routing,
    route_weight,
    expert_gate,
    expert_up,
    expert_down,
    shared_gate,
    shared_up,
    shared_down,
):
    tokens = residual.shape[0]
    width = out_weight.shape[1]
    n_tp = lax.axis_size("tp")
    n_sp = lax.axis_size("sp")
    rows = tokens // n_tp
    experts = n_sp * EXP_DEV
    most = max(1, 2 * rows * TOPK // experts)
    slots = n_tp * most
    total = experts * slots
    cols = expert_down.shape[2]
    product = (in_gate.astype(jnp.float32) * conv_input.astype(jnp.float32)).astype(jnp.bfloat16)
    tail = (product[tokens - CONV_K + 1 :], doc_ids[tokens - CONV_K + 1 :].astype(jnp.bfloat16))
    prev_rows, prev_docs = from_behind((tail[0], tail[1]), "sp", 1)
    extended = jnp.concatenate([prev_rows, product], axis=0).astype(jnp.float32)
    ext_docs = jnp.concatenate([prev_docs.astype(jnp.int32), doc_ids])
    mixed = jnp.zeros(product.shape, jnp.float32)
    for k in range(CONV_K):
        keep = (ext_docs[k : k + tokens] == doc_ids)[:, None]
        mixed = mixed + jnp.where(keep, conv_taps[k] * extended[k : k + tokens], jnp.float32(0.0))
    conv_out = out_gate.astype(jnp.float32) * mixed
    squares = lax.psum(jnp.sum(conv_out * conv_out, axis=1), "tp")
    normed = (conv_out * lax.rsqrt(squares / D_CONV + 1e-06)[:, None] * mix_gain).astype(
        jnp.bfloat16
    )
    partial_value = jnp.dot(normed, out_weight, preferred_element_type=jnp.float32)
    proj = lax.psum_scatter(
        partial_value.astype(jnp.bfloat16), "tp", scatter_dimension=1, tiled=True
    ).astype(jnp.float32)
    stream = (residual.astype(jnp.float32) + proj).astype(jnp.bfloat16)
    stream32 = stream.astype(jnp.float32)
    stream_sq = lax.psum(jnp.sum(stream32 * stream32, axis=1), "tp")
    normal_cols = (stream32 * lax.rsqrt(stream_sq / width + 1e-06)[:, None] * ffn_gain).astype(
        jnp.bfloat16
    )
    flat_expert = routing.reshape(-1)
    onehot = (flat_expert[:, None] == jnp.arange(experts, dtype=jnp.int32)[None, :]).astype(
        jnp.int32
    )
    blocked = onehot.reshape(n_tp, rows * TOPK, experts)
    earlier = jnp.cumsum(blocked, axis=1) - blocked
    position = jnp.sum(earlier * blocked, axis=2).reshape(-1)
    entry = jnp.arange(tokens * TOPK, dtype=jnp.int32)
    slot = flat_expert * slots + entry // (rows * TOPK) * most + position
    table = jnp.full((total,), tokens, jnp.int32).at[slot].set(entry // TOPK)
    block_rows = lax.all_to_all(normal_cols, "tp", split_axis=0, concat_axis=1, tiled=True)
    mine = lax.dynamic_index_in_dim(
        table.reshape(n_sp, EXP_DEV, n_tp, most), lax.axis_index("tp"), 2, False
    )
    local = jnp.where(mine >= tokens, rows, mine - lax.axis_index("tp") * rows)
    padded_block = jnp.concatenate([block_rows, jnp.zeros((1, width), jnp.bfloat16)], axis=0)
    got = lax.all_to_all(padded_block[local], "sp", split_axis=0, concat_axis=0, tiled=True)
    arrived, whole = (
        lax.all_gather(got, "tp", axis=2, tiled=True),
        lax.all_gather(block_rows.reshape(1, 1, rows, width), "tp", axis=2, tiled=True),
    )
    normal = whole.reshape(tokens, width)
    gate = jnp.einsum("nesd,edh->nesh", arrived, expert_gate, preferred_element_type=jnp.float32)
    upper = jnp.einsum("nesd,edh->nesh", arrived, expert_up, preferred_element_type=jnp.float32)
    hidden = (jax.nn.silu(gate) * upper).astype(jnp.bfloat16)
    hidden_flat = hidden.reshape(n_sp * EXP_DEV * slots, hidden.shape[3])
    shared_hid = (
        jax.nn.silu(jnp.dot(normal, shared_gate, preferred_element_type=jnp.float32))
        * jnp.dot(normal, shared_up, preferred_element_type=jnp.float32)
    ).astype(jnp.bfloat16)
    expert_piece = lax.all_gather(hidden_flat, "tp", axis=1, tiled=True)
    shared_piece = lax.all_gather(shared_hid, "tp", axis=1, tiled=True)
    count = expert_piece.shape[1]
    expert_part = jnp.einsum(
        "nesh,ehd->nesd",
        expert_piece.reshape(n_sp, EXP_DEV, slots, count),
        expert_down,
        preferred_element_type=jnp.float32,
    )
    shared_part = jnp.dot(shared_piece, shared_down, preferred_element_type=jnp.float32)
    returned = lax.all_to_all(
        expert_part.astype(jnp.bfloat16), "sp", split_axis=0, concat_axis=0, tiled=True
    )
    picked = (
        returned.reshape(total, cols)[slot].astype(jnp.float32) * route_weight.reshape(-1)[:, None]
    )
    routed = jnp.sum(picked.reshape(tokens, TOPK, cols), axis=1)
    return (stream32 + shared_part + routed).astype(jnp.bfloat16)


MESH = pl.DeviceIdType.MESH
F32 = jnp.float32
BF16 = jnp.bfloat16


def silu_mul(gate, upper):
    return (gate / (1.0 + jnp.exp(-gate)) * upper).astype(BF16)


def mm(a, b):
    return jnp.dot(a, b, preferred_element_type=F32)


SPLIT = 2


def plan(n_z):
    last = n_z - 1
    orders = []
    for z in range(n_z):
        near = sorted((q for q in range(n_z) if q != z), key=lambda q: (abs(q - z), -q if z < n_z / 2 else q))
        orders.append(
            [(q, 0) for q in near] + [(q, 1) for q in reversed(near)] + [(z, 0), (z, 1)]
        )
    others = 2 * last
    base = SPLIT * n_z + 1

    def digit(item):
        return item[0] * SPLIT + item[1] + 1

    def pack(lists, slots):
        codes = []
        for k in range(slots):
            value = 0
            for step in sorted(lists, reverse=True):
                here = lists[step]
                value = value * base + (digit(here[k]) if k < len(here) else 0)
            codes.append(value)
        return codes

    lead, result = 2, []
    for z in range(n_z):
        order = orders[z]
        ends = z in (0, last)
        ahead = {i: [] for i in range(-lead, others + 2 - lead)}
        for k, item in enumerate(order):
            at = k - lead if ends or k >= others else k * 2 // 3 - lead
            ahead[at] = sorted(ahead[at] + [item], key=lambda other: abs(other[0] - z))
        close = {i: [] for i in range(1, others + 3)}
        for k, item in enumerate(order[:others]):
            end = 0 if item[0] > z else last
            at = max(k, orders[end].index(item) + abs(z - end))
            close[at + 1].append(item)
        result.append(
            (
                pack({k: [item] for k, item in enumerate(order)}, 1)
                + pack(ahead, 2)
                + pack(close, 2)
            )
        )
    return result, base


def layer_kernel(
    n_z,
    most,
    og_hbm,
    ig_hbm,
    ci_hbm,
    res_hbm,
    wo_hbm,
    docs_ref,
    taps_ref,
    mix_ref,
    ffn_ref,
    own_meta,
    wg_hbm,
    wu_hbm,
    wd_hbm,
    sg_hbm,
    su_hbm,
    sd_hbm,
    out_ref,
    og,
    ig,
    ci,
    res,
    wo,
    wg,
    wu,
    wd,
    sg,
    su,
    sd,
    ext,
    dext,
    hsend,
    hrecv,
    act,
    ssq,
    srow,
    scl,
    gsend,
    grecv,
    fg,
    tri,
    blk,
    meta,
    xs,
    hid,
    shid,
    ys,
    acc,
    outgo,
    sib,
    back,
    load_sem,
    halo_sem,
    sum_sem,
    fg_sem,
    giv_send,
    giv_recv,
    z_send,
    x_send,
    c_send,
    b_recv,
    m_send,
    m_recv,
    hid_send,
    hid_recv,
    sh_send,
    sh_recv,
    sib_send,
    sib_recv,
    back_send,
    back_recv,
):
    first = [
        pltpu.make_async_copy(src, dst, load_sem.at[n])
        for n, (src, dst) in enumerate(
            ((ig_hbm, ig), (ci_hbm, ci), (og_hbm, og), (wo_hbm, wo), (res_hbm, res))
        )
    ]
    later = [
        pltpu.make_async_copy(src, dst, load_sem.at[5 + n])
        for n, (src, dst) in enumerate(
            ((wg_hbm, wg), (wu_hbm, wu), (wd_hbm, wd), (sg_hbm, sg), (su_hbm, su), (sd_hbm, sd))
        )
    ]
    for load in first:
        load.start()
    s = lax.axis_index("sp")
    t = lax.axis_index("tp")
    z = s // 2
    c = s % 2
    tokens, chan = ig.shape
    cols = out_ref.shape[1]
    width = 2 * cols
    half_rows = tokens // SPLIT
    piece = half_rows // 2
    unit = wg.shape[2]
    pad = ext.shape[0] - tokens
    lo = z > 0
    hi = z < n_z - 1
    up, down = {"sp": s + 2}, {"sp": s - 2}
    other, peer = {"sp": s + 1 - 2 * c}, {"tp": 1 - t}
    after = {"sp": s + 1}
    before = {"sp": s - 1}
    targets = (up, down, peer, other)
    n_items = SPLIT * n_z

    def remote(src, dst, ssem, rsem, dev):
        return pltpu.make_async_remote_copy(
            src_ref=src,
            dst_ref=dst,
            send_sem=ssem,
            recv_sem=rsem,
            device_id=dev,
            device_id_type=MESH,
        )

    def chunk(zq, cq, h, half, q, ssem, dev):
        ref = blk.at[zq * 2 + cq, h, half, pl.ds(q * piece, piece)]
        return remote(ref, ref, ssem, b_recv.at[zq * 2 + cq, h, half, q], dev)

    def z_copy(way, zq, half, q):
        return chunk(zq, c, t, half, q, z_send.at[way, zq, half, q], targets[way])

    def x_copy(zq, half, q):
        return chunk(zq, c, t, half, q, x_send.at[zq, half, q], peer)

    def c_copy(zq, h, half, q):
        return chunk(zq, c, h, half, q, c_send.at[zq, h, half, q], other)

    def arrived(zq, cq, h, half, q):
        chunk(zq, cq, h, half, q, c_send.at[zq, h, half, q], other).wait_recv()

    def m_copy(way, zq, cq):
        b = zq * 2 + cq
        return remote(
            meta.at[b], meta.at[b], m_send.at[way, zq], m_recv.at[b], (up, down, other)[way]
        )

    def hid_copy(zq, half):
        return remote(
            hid.at[t, zq, half],
            hid.at[t, zq, half],
            hid_send.at[zq, half],
            hid_recv.at[zq, half],
            peer,
        )

    def sh_copy(half):
        return remote(
            shid.at[t, half], shid.at[t, half], sh_send.at[half], sh_recv.at[half], peer
        )

    def sib_copy(zq, half):
        return remote(
            outgo.at[zq, half],
            sib.at[zq, half],
            sib_send.at[zq, half],
            sib_recv.at[zq, half],
            other,
        )

    def back_copy(zq, half, q, to, dev):
        return remote(
            acc.at[zq, half, pl.ds(q * piece, piece)],
            back.at[to, half, pl.ds(q * piece, piece)],
            back_send.at[zq, half, q],
            back_recv.at[to, half, q],
            dev,
        )

    def halo_copy():
        return remote(hsend, hrecv, halo_sem.at[0], halo_sem.at[1], after)

    def sum_copy():
        return remote(srow.at[0], srow.at[1], sum_sem.at[0], sum_sem.at[1], peer)

    def fg_copy():
        return remote(fg.at[t], fg.at[t], fg_sem.at[0], fg_sem.at[1], peer)

    def giv_copy(r):
        return remote(gsend.at[r], grecv.at[r], giv_send.at[r], giv_recv.at[r], peer)

    barrier = pltpu.get_barrier_semaphore()
    cross_up = hi & (c == 1)
    cross_down = lo & (c == 0)
    for target, there in ((up, hi), (down, lo), (after, cross_up), (before, cross_down)):

        @pl.when(there)
        def _():
            pl.semaphore_signal(barrier, inc=1, device_id=target, device_id_type=MESH)

    for target in (peer, other):
        pl.semaphore_signal(barrier, inc=1, device_id=target, device_id_type=MESH)

    has_next = s < 2 * n_z - 1
    has_prev = s > 0
    first[0].wait()
    first[1].wait()

    tail = 16

    def product(rows):
        return (ig[rows, :].astype(F32) * ci[rows, :].astype(F32)).astype(BF16).astype(F32)

    end_rows = product(pl.ds(tokens - tail, tail))
    hsend[:, :chan] = end_rows[tail - 8 :]
    hsend[:, chan:] = docs_ref[tokens - 8 :, :]
    fg[t] = jnp.broadcast_to(ffn_ref[...], fg.shape[1:])
    arrivals = (
        2
        + lo.astype(jnp.int32)
        + hi.astype(jnp.int32)
        + cross_up.astype(jnp.int32)
        + cross_down.astype(jnp.int32)
    )
    pl.semaphore_wait(barrier, arrivals)

    @pl.when(has_next)
    def _():
        halo_copy().start()

    fg_copy().start()
    meta[z * 2 + c] = own_meta[...]

    @pl.when(hi)
    def _():
        m_copy(0, z, c).start()

    @pl.when(lo)
    def _():
        m_copy(1, z, c).start()

    m_copy(2, z, c).start()

    step_rows = 32

    @pl.loop(0, tokens // step_rows)
    def _(i):
        at = pl.multiple_of(i * step_rows, step_rows)
        ext[pl.ds(pad + at, step_rows), :] = product(pl.ds(at, step_rows))
        dext[pl.ds(pad + at, step_rows), :] = docs_ref[pl.ds(at, step_rows), :]

    n_tri = tri.shape[0]
    row_id = lax.broadcasted_iota(jnp.int32, (n_tri, n_tri), 0)
    col_id = lax.broadcasted_iota(jnp.int32, (n_tri, n_tri), 1)
    tri[...] = (row_id < col_id).astype(F32).astype(BF16)
    for load in first[2:]:
        load.wait()
    for load in later:
        load.start()

    @pl.when(has_prev)
    def _():
        halo_copy().wait_recv()
        ext[pad - 8 : pad, :] = hrecv[:, :chan]
        dext[pad - 8 : pad, :] = hrecv[:, chan:]

    @pl.when(jnp.logical_not(has_prev))
    def _():
        ext[pad - 8 : pad, :] = jnp.zeros((8, chan), F32)
        dext[pad - 8 : pad, :] = jnp.zeros((8, dext.shape[1]), F32)

    lanes = dext.shape[1]

    @pl.loop(0, tokens // step_rows)
    def _(i):
        at = pl.multiple_of(i * step_rows, step_rows)
        v = ext[pl.ds(pl.multiple_of(pad - 8 + at, 8), step_rows + 8), :]
        d = dext[pl.ds(pl.multiple_of(pad - 8 + at, 8), step_rows + 8), :]
        doc = d[8:]
        mixed = None
        for k in range(CONV_K):
            by = CONV_K - 1 - k
            if by:
                same = (pltpu.roll(d, by, 0)[8:] == doc).astype(F32)
                same = jnp.concatenate([same] * (chan // lanes), axis=1)
                term = taps_ref[k : k + 1, :] * pltpu.roll(v, by, 0)[8:] * same
            else:
                term = taps_ref[k : k + 1, :] * v[8:]
            mixed = term if mixed is None else mixed + term
        rows = pl.ds(at, step_rows)
        conv_out = og[rows, :].astype(F32) * mixed
        total = jnp.sum(conv_out * conv_out, axis=1, keepdims=True)
        ssq[rows, :] = jnp.broadcast_to(total, (step_rows, lanes))
        act[rows, :] = (conv_out * mix_ref[...]).astype(BF16)

    eye = lax.broadcasted_iota(jnp.int32, (lanes, lanes), 0) == lax.broadcasted_iota(
        jnp.int32, (lanes, lanes), 1
    )
    for k in range(tokens // lanes):
        part = ssq[k * lanes : (k + 1) * lanes, :]
        line = jnp.sum(jnp.where(eye, part, F32(0.0)), axis=0, keepdims=True)
        srow[0, :, k * lanes : (k + 1) * lanes] = jnp.broadcast_to(line, (8, lanes))
    sum_copy().start()

    n_chunks = 2 * SPLIT

    def out_cols(who):
        return pl.ds(pl.multiple_of(who * cols, cols), cols)

    for r in range(n_chunks):
        gsend[r] = mm(act[r * piece : (r + 1) * piece, :], wo[:, out_cols(1 - t)]).astype(BF16)
        giv_copy(r).start()

    sum_copy().wait_recv()
    for k in range(tokens // lanes):
        line = srow[1, 0:1, k * lanes : (k + 1) * lanes]
        theirs = jnp.sum(jnp.where(eye, line, F32(0.0)), axis=1, keepdims=True)
        whole = ssq[k * lanes : (k + 1) * lanes, :] + theirs
        scl[k * lanes : (k + 1) * lanes, :] = lax.rsqrt(whole / (2 * chan) + 1e-06)

    for r in range(n_chunks):
        half, q = divmod(r, 2)
        rows = slice(r * piece, (r + 1) * piece)
        kept = mm(act[rows, :], wo[:, out_cols(t)])
        giv_copy(r).wait_recv()
        proj = (kept + grecv[r].astype(F32)) * scl[rows, 0:1]
        blk[z * 2 + c, t, half, q * piece : (q + 1) * piece, :] = (
            res[rows, :].astype(F32) + proj
        ).astype(BF16)

        if half == 0:
            go_up, go_down = hi, lo
        else:
            go_up, go_down = hi & jnp.logical_not(lo), lo & jnp.logical_not(hi)

        @pl.when(go_up)
        def _():
            z_copy(0, z, half, q).start()

        @pl.when(go_down)
        def _():
            z_copy(1, z, half, q).start()

        c_copy(z, t, half, q).start()

    fg_copy().wait_recv()
    for load in later:
        load.wait()

    def picks(zq, cq, half):
        info = meta[zq * 2 + cq, half][:, :half_rows]
        mine = (lax.broadcasted_iota(jnp.int32, (8, half_rows), 0) + s * EXP_DEV).astype(F32)
        hot0 = info[0:1] == mine
        hot1 = info[1:2] == mine
        hot = hot0 | hot1
        earlier = mm(hot.astype(F32).astype(BF16), tri[...])
        position = jnp.where(hot, earlier, F32(-1.0))
        weight = jnp.where(hot0, info[2:3], F32(0.0)) + jnp.where(hot1, info[3:4], F32(0.0))
        place = lax.broadcasted_iota(jnp.int32, (most, half_rows), 0).astype(F32)
        chosen = [(position[e : e + 1] == place).astype(F32) for e in range(EXP_DEV)]
        return chosen, weight

    def norm_scale(parts):
        total = sum(jnp.sum(part * part, axis=1, keepdims=True) for part in parts)
        return lax.rsqrt(total / width + 1e-06)

    def normal_of(parts):
        scale = norm_scale(parts)
        return [(part * scale * fg[h, 0:1, :]).astype(BF16) for h, part in enumerate(parts)]

    def sides():
        return [(0, c), (1, 1 - c)]

    def hidden(zq, half):
        for p, cq in sides():
            chosen, _ = picks(zq, cq, half)
            sel = jnp.concatenate(chosen, axis=0).astype(BF16)
            got = normal_of([mm(sel, blk[zq * 2 + cq, h, half]) for h in range(2)])
            for h in range(2):
                for e in range(EXP_DEV):
                    xs[e, p * most : (p + 1) * most, h * cols : (h + 1) * cols] = got[h][
                        e * most : (e + 1) * most
                    ]
        for e in range(EXP_DEV):
            hid[t, zq, half, e] = silu_mul(mm(xs[e], wg[e]), mm(xs[e], wu[e]))

    def shared(half):
        whole = normal_of([blk[z * 2 + c, h, half].astype(F32) for h in range(2)])
        gate = mm(whole[0], sg[:cols, :]) + mm(whole[1], sg[cols:, :])
        upper = mm(whole[0], su[:cols, :]) + mm(whole[1], su[cols:, :])
        shid[t, half] = silu_mul(gate, upper)

    def results(zq, half):
        hid_copy(zq, half).wait_recv()
        for e in range(EXP_DEV):
            ys[e] = (
                mm(hid[0, zq, half, e], wd[e, :unit, :]) + mm(hid[1, zq, half, e], wd[e, unit:, :])
            ).astype(BF16)
        for p, cq in sides():
            chosen, weight = picks(zq, cq, half)
            parts = []
            for e in range(EXP_DEV):
                scale = jnp.sum(chosen[e] * weight[e : e + 1], axis=1, keepdims=True)
                part = ys[e, p * most : (p + 1) * most, :].astype(F32)
                parts.append((part * scale).astype(BF16))
            sel = jnp.concatenate(chosen, axis=0).astype(BF16)
            into = acc if p == 0 else outgo
            into[zq, half] = lax.dot_general(
                sel,
                jnp.concatenate(parts, axis=0),
                (((0,), (0,)), ((), ())),
                preferred_element_type=F32,
            ).astype(BF16)
        sib_copy(zq, half).start()

    def is_end(zq):
        return ((zq > z) & jnp.logical_not(lo)) | ((zq < z) & jnp.logical_not(hi))

    def combine(zq, half):
        sib_copy(zq, half).wait_recv()
        end = is_end(zq)
        for q in range(2):
            rows = slice(q * piece, (q + 1) * piece)

            @pl.when(end)
            def _():
                acc[zq, half, rows, :] = (
                    acc[zq, half, rows, :].astype(F32) + sib[zq, half, rows, :].astype(F32)
                ).astype(BF16)

            @pl.when(jnp.logical_not(end))
            def _():
                back_copy(zq, half, q, zq, up).wait_recv()
                acc[zq, half, rows, :] = (
                    acc[zq, half, rows, :].astype(F32)
                    + sib[zq, half, rows, :].astype(F32)
                    + back[zq, half, rows, :].astype(F32)
                ).astype(BF16)

            @pl.when(zq > z)
            def _():
                back_copy(zq, half, q, zq, up).start()

            @pl.when(zq < z - 1)
            def _():
                back_copy(zq, half, q, zq, down).start()

            @pl.when(zq == z - 1)
            def _():
                back_copy(zq, half, q, n_z, down).start()

    def pass_ahead(zq, half):
        @pl.when((zq != z) & (half == 0))
        def _():
            m_copy(2, zq, c).wait_recv()

            @pl.when((zq < z) & hi)
            def _():
                m_copy(0, zq, c).start()

            @pl.when((zq > z) & lo)
            def _():
                m_copy(1, zq, c).start()

            m_copy(2, zq, c).start()

        for q in range(2):

            @pl.when(zq != z)
            def _():
                arrived(zq, c, t, half, q)

                @pl.when((zq < z) & hi)
                def _():
                    z_copy(0, zq, half, q).start()

                @pl.when((zq > z) & lo)
                def _():
                    z_copy(1, zq, half, q).start()

                c_copy(zq, t, half, q).start()

            x_copy(zq, half, q).start()

        @pl.when((zq == z - 1) & (half == 1) & hi)
        def _():
            for q in range(2):
                z_copy(0, z, 1, q).start()

        @pl.when((zq == z + 1) & (half == 1) & lo)
        def _():
            for q in range(2):
                z_copy(1, z, 1, q).start()

    def pass_across(zq, half):
        for q in range(2):
            arrived(zq, c, 1 - t, half, q)
            c_copy(zq, 1 - t, half, q).start()

    def gathered(zq, half):
        @pl.when(half == 0)
        def _():
            m_copy(2, zq, 1 - c).wait_recv()

        for h in range(2):
            for q in range(2):
                arrived(zq, 1 - c, h, half, q)

    def item(code):
        return (code - 1) // SPLIT, (code - 1) % SPLIT

    tables, base = plan(n_z)
    codes = []
    for k in range(len(tables[0])):
        value = 0
        for zz in range(n_z):
            value = value + (z == zz).astype(jnp.int32) * tables[zz][k]
        codes.append(value)

    def turn(i, carry):
        now, ahead0, ahead1, close0, close1, prev = carry
        here = i >= 2
        cur = jnp.where(here, now % base, 0)

        @pl.when(cur > 0)
        def _():
            pass_across(*item(cur))

        @pl.when(prev > 0)
        def _():
            results(*item(prev))

        @pl.when(cur > 0)
        def _():
            zq, half = item(cur)
            gathered(zq, half)
            hidden(zq, half)
            hid_copy(zq, half).start()

            @pl.when(zq == z)
            def _():
                shared(half)
                sh_copy(half).start()

        @pl.loop(0, 2)
        def _(k):
            code = ahead0 % base * (1 - k) + ahead1 % base * k

            @pl.when(code > 0)
            def _():
                pass_ahead(*item(code))

        closing = i >= 3

        @pl.when(closing)
        def _():
            @pl.loop(0, 2)
            def _(k):
                code = close0 % base * (1 - k) + close1 % base * k

                @pl.when(code > 0)
                def _():
                    combine(*item(code))

        def shift(value, live):
            return jnp.where(live, value // base, value)

        return (
            shift(now, here),
            ahead0 // base,
            ahead1 // base,
            shift(close0, closing),
            shift(close1, closing),
            cur,
        )

    lax.fori_loop(0, n_items + 3, turn, tuple(codes) + (jnp.int32(0),))

    for half in range(SPLIT):
        sib_copy(z, half).wait_recv()
        sh_copy(half).wait_recv()
        for q in range(2):

            @pl.when(lo)
            def _():
                back_copy(z, half, q, z, up).wait_recv()

            @pl.when(hi)
            def _():
                back_copy(z, half, q, n_z, up).wait_recv()

            rows = slice(q * piece, (q + 1) * piece)
            fin = (
                blk[z * 2 + c, t, half, rows, :].astype(F32)
                + mm(shid[0, half, rows, :], sd[:unit, :])
                + mm(shid[1, half, rows, :], sd[unit:, :])
                + acc[z, half, rows, :].astype(F32)
                + sib[z, half, rows, :].astype(F32)
            )
            low = jnp.where(lo, back[z, half, rows, :].astype(F32), F32(0.0))
            high = jnp.where(hi, back[n_z, half, rows, :].astype(F32), F32(0.0))
            at = half * half_rows + q * piece
            out_ref[at : at + piece, :] = (fin + low + high).astype(BF16)

    @pl.when(has_next)
    def _():
        halo_copy().wait_send()

    fg_copy().wait_send()
    sum_copy().wait_send()
    for r in range(n_chunks):
        giv_copy(r).wait_send()
    for half in range(SPLIT):
        sh_copy(half).wait_send()

    @pl.loop(0, n_z)
    def _(zq):
        @pl.when(hi & (zq <= z))
        def _():
            m_copy(0, zq, c).wait_send()
            for half in range(SPLIT):
                for q in range(2):
                    z_copy(0, zq, half, q).wait_send()

        @pl.when(lo & (zq >= z))
        def _():
            m_copy(1, zq, c).wait_send()
            for half in range(SPLIT):
                for q in range(2):
                    z_copy(1, zq, half, q).wait_send()

        m_copy(2, zq, c).wait_send()
        for half in range(SPLIT):
            for q in range(2):
                x_copy(zq, half, q).wait_send()
                for h in range(2):
                    c_copy(zq, h, half, q).wait_send()

                @pl.when(zq != z)
                def _():
                    back_copy(zq, half, q, zq, up).wait_send()

            hid_copy(zq, half).wait_send()
            sib_copy(zq, half).wait_send()


def fast(
    out_gate,
    in_gate,
    conv_input,
    doc_ids,
    residual,
    conv_taps,
    mix_gain,
    out_weight,
    ffn_gain,
    routing,
    route_weight,
    expert_gate,
    expert_up,
    expert_down,
    shared_gate,
    shared_up,
    shared_down,
):
    tokens, cols = residual.shape
    chan, width = out_weight.shape
    n_tp, n_sp = lax.axis_size("tp"), lax.axis_size("sp")
    n_z = n_sp // 2
    rows = tokens // n_tp
    experts = n_sp * EXP_DEV
    most = max(1, 2 * rows * TOPK // experts)
    lanes = 128
    docs = jnp.broadcast_to(doc_ids.astype(F32)[:, None], (tokens, lanes))
    info = jnp.concatenate([routing.astype(F32), route_weight], axis=1)
    info = info.reshape(SPLIT, rows, 2 * TOPK).transpose(0, 2, 1)
    info = jnp.pad(info, ((0, 0), (0, 8 - 2 * TOPK), (0, -rows % lanes)), constant_values=-1.0)

    piece = rows // 2
    blocks = n_sp
    unit = expert_gate.shape[2]
    vm = pl.BlockSpec(memory_space=pltpu.VMEM)
    hbm = pl.BlockSpec(memory_space=pl.ANY)
    dma = pltpu.SemaphoreType.DMA
    return pl.pallas_call(
        functools.partial(layer_kernel, n_z, most),
        out_shape=jax.ShapeDtypeStruct((tokens, cols), BF16),
        in_specs=[hbm] * 5 + [vm] * 5 + [hbm] * 6,
        out_specs=vm,
        scratch_shapes=[
            pltpu.VMEM((tokens, chan), BF16),
            pltpu.VMEM((tokens, chan), BF16),
            pltpu.VMEM((tokens, chan), BF16),
            pltpu.VMEM((tokens, cols), BF16),
            pltpu.VMEM((chan, width), BF16),
            pltpu.VMEM(expert_gate.shape, BF16),
            pltpu.VMEM(expert_up.shape, BF16),
            pltpu.VMEM(expert_down.shape, BF16),
            pltpu.VMEM(shared_gate.shape, BF16),
            pltpu.VMEM(shared_up.shape, BF16),
            pltpu.VMEM(shared_down.shape, BF16),
            pltpu.VMEM((tokens + 16, chan), F32),
            pltpu.VMEM((tokens + 16, lanes), F32),
            pltpu.VMEM((8, chan + lanes), F32),
            pltpu.VMEM((8, chan + lanes), F32),
            pltpu.VMEM((tokens, chan), BF16),
            pltpu.VMEM((tokens, lanes), F32),
            pltpu.VMEM((2, 8, tokens), F32),
            pltpu.VMEM((tokens, lanes), F32),
            pltpu.VMEM((2 * SPLIT, piece, cols), BF16),
            pltpu.VMEM((2 * SPLIT, piece, cols), BF16),
            pltpu.VMEM((2, 8, cols), F32),
            pltpu.VMEM((rows, rows), BF16),
            pltpu.VMEM((blocks, 2, SPLIT, rows, cols), BF16),
            pltpu.VMEM((blocks,) + info.shape, F32),
            pltpu.VMEM((EXP_DEV, 2 * most, width), BF16),
            pltpu.VMEM((2, n_z, SPLIT, EXP_DEV, 2 * most, unit), BF16),
            pltpu.VMEM((2, SPLIT, rows, unit), BF16),
            pltpu.VMEM((EXP_DEV, 2 * most, cols), BF16),
            pltpu.VMEM((n_z, SPLIT, rows, cols), BF16),
            pltpu.VMEM((n_z, SPLIT, rows, cols), BF16),
            pltpu.VMEM((n_z, SPLIT, rows, cols), BF16),
            pltpu.VMEM((n_z + 1, SPLIT, rows, cols), BF16),
            dma((11,)),
            dma((2,)),
            dma((2,)),
            dma((2,)),
            dma((2 * SPLIT,)),
            dma((2 * SPLIT,)),
            dma((2, n_z, SPLIT, 2)),
            dma((n_z, SPLIT, 2)),
            dma((n_z, 2, SPLIT, 2)),
            dma((blocks, 2, SPLIT, 2)),
            dma((3, n_z)),
            dma((blocks,)),
            dma((n_z, SPLIT)),
            dma((n_z, SPLIT)),
            dma((SPLIT,)),
            dma((SPLIT,)),
            dma((n_z, SPLIT)),
            dma((n_z, SPLIT)),
            dma((n_z, SPLIT, 2)),
            dma((n_z + 1, SPLIT, 2)),
        ],
        compiler_params=pltpu.CompilerParams(
            collective_id=0, has_side_effects=True, vmem_limit_bytes=64 * 1024 * 1024 - 65536
        ),
    )(
        out_gate,
        in_gate,
        conv_input,
        residual,
        out_weight,
        docs,
        conv_taps,
        mix_gain[None, :],
        ffn_gain[None, :],
        info,
        expert_gate,
        expert_up,
        expert_down,
        shared_gate,
        shared_up,
        shared_down,
    )


def fits(mesh):
    return mesh.shape["tp"] == 2 and mesh.shape["sp"] in (4, 6, 8)


def solution(mesh):
    return jax.shard_map(
        fast if fits(mesh) else body,
        mesh=mesh,
        in_specs=(
            P(("grp", "sp"), "tp"),
            P(("grp", "sp"), "tp"),
            P(("grp", "sp"), "tp"),
            P(("grp", "sp")),
            P(("grp", "sp"), "tp"),
            P(None, "tp"),
            P("tp"),
            P("tp", None),
            P("tp"),
            P(("grp", "sp"), None),
            P(("grp", "sp"), None),
            P("sp", None, "tp"),
            P("sp", None, "tp"),
            P("sp", None, "tp"),
            P(None, "tp"),
            P(None, "tp"),
            P(None, "tp"),
        ),
        out_specs=P(("grp", "sp"), "tp"),
        check_vma=False,
    )
```

time: 192 us -> 136 us (0.71)
  the two profiles are of different devices: /device:TPU:0 before, /device:TPU:13 now
where the time goes in v1:
time: 136 us
  Pallas kernels  130 us (96%)
  local copies, waits for them, and re-layouts  3.56 us (3%)
  other arithmetic  2.06 us (2%)
    pallas_call x1, Pallas kernels, fast(): pl.pallas_call(functools.partial(layer_kernel, n_z, most), out_shape=jax....  130 us

profile of v1, /device:TPU:13, one launch (start us, length us, event | category | flops | bytes accessed | tf_op | source)
XLA Modules:
  0.0 135.9 jit_solution(8619239238717004352)
XLA Ops:
  0.0 0.7 convert_element_type.6
  0.7 0.7 convert_element_type.7
  1.4 0.7 pad_maximum_fusion
  2.1 0.1 reshape.4
  2.2 0.6 pad.4.own_meta
  2.8 0.8 broadcast_in_dim.12.docs_ref
  3.6 130.3 %shard_map.163 = bf16[384,1024]{1,0:T(8,128)(2,1)} custom-call(bf16[384,512]{1,0:T(8,128)(2,1)} %og_hbm.1, bf16[384,512]{1,0:T(8,128)(2,1)} %ig_hbm.1, bf16[384,512]{1,0:T(8,128)(2,1)} %ci_hbm.1, bf16[384,1024]{1,0:T(8,128)(2,1)} %res_hbm.1, bf16[512,2048]{1,0:T(8,128)(2,1)} %wo_hbm.1, f32[384,128]{1,0:T(8,128)} %broadcast_in_dim.12.docs_ref, ...), custom_call_target="tpu_custom_call" | custom-call | tf_op jit(solution)/shard_map/pallas_call | solution.py:865
  133.9 2.1 %copy.22 = bf16[384,1024]{1,0:T(8,128)(2,1)} copy(bf16[384,1024]{1,0:T(8,128)(2,1)} %shard_map.163) | data formatting | bytes 1572864
  (1 shorter events, 0.0 us)

commit v2 on v1

--- a/solution.py
+++ b/solution.py
@@ -138,51 +138,134 @@
 SPLIT = 2
 
 
+FULL = ((0, 1), (0, 1))
+HOP, START, DEPTH = 2.8, 6.0, 1.0
+W = (8.4, 6.0, 3.8, -3.3, 5.9, 4.9, 4.7, -4.7, -0.8, 1.6, 5.9, 3.4, 5.6)
+KINDS = ("stream", "land", "up", "down", "across", "hidden", "result", "combine")
+
+
+def full_rows(n_z, source, target, half, q):
+    return abs(source - target) == 1 and half * 2 + q in FULL[0 < target < n_z - 1]
+
+
 def plan(n_z):
-    last = n_z - 1
-    orders = []
-    for z in range(n_z):
-        near = sorted((q for q in range(n_z) if q != z), key=lambda q: (abs(q - z), -q if z < n_z / 2 else q))
-        orders.append(
-            [(q, 0) for q in near] + [(q, 1) for q in reversed(near)] + [(z, 0), (z, 1)]
-        )
-    others = 2 * last
-    base = SPLIT * n_z + 1
-
-    def digit(item):
-        return item[0] * SPLIT + item[1] + 1
-
-    def pack(lists, slots):
-        codes = []
-        for k in range(slots):
-            value = 0
-            for step in sorted(lists, reverse=True):
-                here = lists[step]
-                value = value * base + (digit(here[k]) if k < len(here) else 0)
-            codes.append(value)
-        return codes
-
-    lead, result = 2, []
-    for z in range(n_z):
-        order = orders[z]
-        ends = z in (0, last)
-        ahead = {i: [] for i in range(-lead, others + 2 - lead)}
-        for k, item in enumerate(order):
-            at = k - lead if ends or k >= others else k * 2 // 3 - lead
-            ahead[at] = sorted(ahead[at] + [item], key=lambda other: abs(other[0] - z))
-        close = {i: [] for i in range(1, others + 3)}
-        for k, item in enumerate(order[:others]):
-            end = 0 if item[0] > z else last
-            at = max(k, orders[end].index(item) + abs(z - end))
-            close[at + 1].append(item)
-        result.append(
-            (
-                pack({k: [item] for k, item in enumerate(order)}, 1)
-                + pack(ahead, 2)
-                + pack(close, 2)
-            )
-        )
-    return result, base
+    wire, hop, near = 4.2, HOP, 1.6
+    cost = dict(
+        stream=0.35, land=0.1, up=0.1, down=0.1, across=0.1, hidden=1.7, result=1.35, combine=0.3
+    )
+    chunks = [(half, q) for half in range(SPLIT) for q in range(2)]
+    zones = range(n_z)
+    have, told, heard, summed, went = {}, {}, {}, {}, {}
+    todo = {z: [] for z in zones}
+    for z in zones:
+        for k, (half, q) in enumerate(chunks):
+            todo[z].append(("stream", z, 0, half, q))
+            went[z, z, half, q] = START + wire * (k + 1) + hop
+        for zq in zones:
+            for half, q in chunks:
+                if zq != z:
+                    todo[z].append(("land", zq, 0, half, q))
+                todo[z].append(("land", zq, 1, half, q))
+                if zq <= z < n_z - 1:
+                    todo[z].append(("up", zq, 0, half, q))
+                if zq >= z > 0:
+                    todo[z].append(("down", zq, 0, half, q))
+                if not full_rows(n_z, zq, z, half, q):
+                    todo[z].append(("across", zq, 0, half, q))
+            for half in range(SPLIT):
+                todo[z].append(("hidden", zq, 0, half, 0))
+                todo[z].append(("result", zq, 0, half, 0))
+                if zq != z:
+                    todo[z] += [("combine", zq, 0, half, q) for q in range(2)]
+        for half, q in chunks:
+            if z < n_z - 1 and full_rows(n_z, z, z + 1, half, q):
+                todo[z].append(("up", z, 1, half, q))
+            if z > 0 and full_rows(n_z, z, z - 1, half, q):
+                todo[z].append(("down", z, 1, half, q))
+    arrive = {}
+    link = {(z, way): 0.0 for z in zones for way in ("up", "down", "across")}
+    for z in zones:
+        link[z, "across"] = START + wire * len(chunks)
+    core = {z: 0.0 for z in zones}
+    never = 1e9
+
+    def put(z, way, now, size):
+        begin = max(now, link[z, way])
+        link[z, way] = begin + wire * size
+        return link[z, way] + hop
+
+    def ready(z, event):
+        kind, zq, h, half, q = event
+        if kind == "stream":
+            return went[z, z, half, q]
+        if kind == "land":
+            return arrive.get((z, zq, h, half, q), never)
+        if kind in ("up", "down", "across"):
+            return max(have.get((z, zq, h, half, q), never), link[z, kind] - DEPTH)
+        if kind == "hidden":
+            return max(have.get((z, zq, g, half, p), never) for g in range(2) for p in range(2)) + near
+        if kind == "result":
+            return heard.get((z, zq, half), never)
+        before = z - 1 if zq > z else z + 1
+        coming = summed.get((before, zq, half, q), never) if 0 <= before < n_z else 0.0
+        return max(told.get((z, zq, half), never), coming)
+
+    def rank(z, event):
+        kind, zq, h, half, q = event
+        away = abs(zq - z)
+        if kind in ("stream", "land"):
+            return (0, 0.0)
+        if kind == "combine":
+            return (1, W[12] * away + half)
+        if kind in ("result", "hidden"):
+            return (2, (kind == "hidden") * 1.0, W[11] * away)
+        if kind == "across":
+            return (3, W[away] + W[4] * half, q)
+        return (3, (W[9] if h else W[5 + away]) + W[10] * half, q)
+
+    order = {z: [] for z in zones}
+    while any(todo.values()):
+        best = None
+        for z in zones:
+            if not todo[z]:
+                continue
+            starts = [(max(core[z], ready(z, event)), event) for event in todo[z]]
+            at = min(start for start, _ in starts)
+            if best is None or at < best[0]:
+                best = (at, z, starts)
+        at, z, starts = best
+        assert at < never
+        event = min((e for start, e in starts if start <= at), key=lambda e: rank(z, e))
+        kind, zq, h, half, q = event
+        todo[z].remove(event)
+        order[z].append(event)
+        end = at + cost[kind] + (0.9 if kind == "hidden" and zq == z else 0.0)
+        core[z] = end
+        if kind in ("stream", "land"):
+            have[z, zq, h, half, q] = end
+        elif kind in ("up", "down"):
+            arrive[z + (1 if kind == "up" else -1), zq, h, half, q] = put(z, kind, end, 1)
+        elif kind == "across":
+            arrive[z, zq, 1, half, q] = put(z, kind, end, 1)
+        elif kind == "hidden":
+            heard[z, zq, half] = put(z, "across", end, 1.0 if zq == z else 0.5)
+        elif kind == "result":
+            told[z, zq, half] = end + 2.2
+        else:
+            summed[z, zq, half, q] = put(z, "up" if zq > z else "down", end, 1)
+    done = max(max(core.values()), max(summed.values()))
+    return order, done
+
+
+def encode(events):
+    codes = [
+        (((KINDS.index(kind) * 4 + zq) * 2 + h) * 2 + half) * 2 + q
+        for kind, zq, h, half, q in events
+    ]
+    return [
+        sum(code << (8 * k) for k, code in enumerate(codes[at : at + 3]))
+        for at in range(0, len(codes), 3)
+    ]
 
 
 def layer_kernel(
@@ -197,7 +280,8 @@
     taps_ref,
     mix_ref,
     ffn_ref,
-    own_meta,
+    names_ref,
+    share_ref,
     wg_hbm,
     wu_hbm,
     wd_hbm,
@@ -291,7 +375,6 @@
     after = {"sp": s + 1}
     before = {"sp": s - 1}
     targets = (up, down, peer, other)
-    n_items = SPLIT * n_z
 
     def remote(src, dst, ssem, rsem, dev):
         return pltpu.make_async_remote_copy(
@@ -307,8 +390,13 @@
         ref = blk.at[zq * 2 + cq, h, half, pl.ds(q * piece, piece)]
         return remote(ref, ref, ssem, b_recv.at[zq * 2 + cq, h, half, q], dev)
 
-    def z_copy(way, zq, half, q):
-        return chunk(zq, c, t, half, q, z_send.at[way, zq, half, q], targets[way])
+    def side(h):
+        return t + h * (1 - 2 * t)
+
+    def z_copy(way, zq, h, half, q):
+        return chunk(
+            zq, c, side(h), half, q, z_send.at[way, zq + h * (n_z - zq), half, q], targets[way]
+        )
 
     def x_copy(zq, half, q):
         return chunk(zq, c, t, half, q, x_send.at[zq, half, q], peer)
@@ -319,10 +407,14 @@
     def arrived(zq, cq, h, half, q):
         chunk(zq, cq, h, half, q, c_send.at[zq, h, half, q], other).wait_recv()
 
-    def m_copy(way, zq, cq):
-        b = zq * 2 + cq
+    def m_copy(way, zq, cq, half):
+        ref = meta.at[zq * 2 + cq, half]
         return remote(
-            meta.at[b], meta.at[b], m_send.at[way, zq], m_recv.at[b], (up, down, other)[way]
+            ref,
+            ref,
+            m_send.at[way, zq, half],
+            m_recv.at[zq * 2 + cq, half],
+            (up, down, other)[way],
         )
 
     def hid_copy(zq, half):
@@ -339,12 +431,13 @@
             shid.at[t, half], shid.at[t, half], sh_send.at[half], sh_recv.at[half], peer
         )
 
-    def sib_copy(zq, half):
+    def sib_copy(zq, half, q):
+        rows = pl.ds(q * piece, piece)
         return remote(
-            outgo.at[zq, half],
-            sib.at[zq, half],
-            sib_send.at[zq, half],
-            sib_recv.at[zq, half],
+            outgo.at[zq, half, rows],
+            sib.at[zq, half, rows],
+            sib_send.at[zq, half, q],
+            sib_recv.at[zq, half, q],
             other,
         )
 
@@ -391,9 +484,29 @@
     def product(rows):
         return (ig[rows, :].astype(F32) * ci[rows, :].astype(F32)).astype(BF16).astype(F32)
 
+    lanes = dext.shape[1]
+    eye = lax.broadcasted_iota(jnp.int32, (lanes, lanes), 0) == lax.broadcasted_iota(
+        jnp.int32, (lanes, lanes), 1
+    )
+
+    def upright(line):
+        return jnp.sum(jnp.where(eye, line, F32(0.0)), axis=1, keepdims=True)
+
+    docs = docs_ref[...].astype(F32)
+    for k in range(tokens // lanes):
+        column = upright(docs[:, k * lanes : (k + 1) * lanes])
+        dext[pad + k * lanes : pad + (k + 1) * lanes, :] = jnp.broadcast_to(column, (lanes, lanes))
     end_rows = product(pl.ds(tokens - tail, tail))
     hsend[:, :chan] = end_rows[tail - 8 :]
-    hsend[:, chan:] = docs_ref[tokens - 8 :, :]
+    hsend[:, chan:] = dext[pad + tokens - 8 : pad + tokens, :]
+    own = z * 2 + c
+    names = names_ref[...].astype(F32)
+    share = share_ref[...]
+    for half in range(SPLIT):
+        part = slice(half * half_rows, (half + 1) * half_rows)
+        meta[own, half] = jnp.zeros(meta.shape[2:], F32)
+        meta[own, half, 0:TOPK, :half_rows] = names[:, part]
+        meta[own, half, TOPK : 2 * TOPK, :half_rows] = share[:, part]
     fg[t] = jnp.broadcast_to(ffn_ref[...], fg.shape[1:])
     arrivals = (
         2
@@ -409,17 +522,8 @@
         halo_copy().start()
 
     fg_copy().start()
-    meta[z * 2 + c] = own_meta[...]
-
-    @pl.when(hi)
-    def _():
-        m_copy(0, z, c).start()
-
-    @pl.when(lo)
-    def _():
-        m_copy(1, z, c).start()
-
-    m_copy(2, z, c).start()
+    for half in range(SPLIT):
+        m_copy(2, z, c, half).start()
 
     step_rows = 32
 
@@ -427,7 +531,6 @@
     def _(i):
         at = pl.multiple_of(i * step_rows, step_rows)
         ext[pl.ds(pad + at, step_rows), :] = product(pl.ds(at, step_rows))
-        dext[pl.ds(pad + at, step_rows), :] = docs_ref[pl.ds(at, step_rows), :]
 
     n_tri = tri.shape[0]
     row_id = lax.broadcasted_iota(jnp.int32, (n_tri, n_tri), 0)
@@ -448,8 +551,6 @@
     def _():
         ext[pad - 8 : pad, :] = jnp.zeros((8, chan), F32)
         dext[pad - 8 : pad, :] = jnp.zeros((8, dext.shape[1]), F32)
-
-    lanes = dext.shape[1]
 
     @pl.loop(0, tokens // step_rows)
     def _(i):
@@ -473,9 +574,6 @@
         ssq[rows, :] = jnp.broadcast_to(total, (step_rows, lanes))
         act[rows, :] = (conv_out * mix_ref[...]).astype(BF16)
 
-    eye = lax.broadcasted_iota(jnp.int32, (lanes, lanes), 0) == lax.broadcasted_iota(
-        jnp.int32, (lanes, lanes), 1
-    )
     for k in range(tokens // lanes):
         part = ssq[k * lanes : (k + 1) * lanes, :]
         line = jnp.sum(jnp.where(eye, part, F32(0.0)), axis=0, keepdims=True)
@@ -494,34 +592,8 @@
     sum_copy().wait_recv()
     for k in range(tokens // lanes):
         line = srow[1, 0:1, k * lanes : (k + 1) * lanes]
-        theirs = jnp.sum(jnp.where(eye, line, F32(0.0)), axis=1, keepdims=True)
-        whole = ssq[k * lanes : (k + 1) * lanes, :] + theirs
+        whole = ssq[k * lanes : (k + 1) * lanes, :] + upright(line)
         scl[k * lanes : (k + 1) * lanes, :] = lax.rsqrt(whole / (2 * chan) + 1e-06)
-
-    for r in range(n_chunks):
-        half, q = divmod(r, 2)
-        rows = slice(r * piece, (r + 1) * piece)
-        kept = mm(act[rows, :], wo[:, out_cols(t)])
-        giv_copy(r).wait_recv()
-        proj = (kept + grecv[r].astype(F32)) * scl[rows, 0:1]
-        blk[z * 2 + c, t, half, q * piece : (q + 1) * piece, :] = (
-            res[rows, :].astype(F32) + proj
-        ).astype(BF16)
-
-        if half == 0:
-            go_up, go_down = hi, lo
-        else:
-            go_up, go_down = hi & jnp.logical_not(lo), lo & jnp.logical_not(hi)
-
-        @pl.when(go_up)
-        def _():
-            z_copy(0, z, half, q).start()
-
-        @pl.when(go_down)
-        def _():
-            z_copy(1, z, half, q).start()
-
-        c_copy(z, t, half, q).start()
 
     fg_copy().wait_recv()
     for load in later:
@@ -591,175 +663,139 @@
                 (((0,), (0,)), ((), ())),
                 preferred_element_type=F32,
             ).astype(BF16)
-        sib_copy(zq, half).start()
+        for q in range(2):
+            sib_copy(zq, half, q).start()
 
     def is_end(zq):
         return ((zq > z) & jnp.logical_not(lo)) | ((zq < z) & jnp.logical_not(hi))
 
-    def combine(zq, half):
-        sib_copy(zq, half).wait_recv()
+    def strip(q):
+        return pl.ds(pl.multiple_of(q * piece, piece), piece)
+
+    def on_stream(zq, h, half, q):
+        r = half * 2 + q
+        rows = pl.ds(pl.multiple_of(r * piece, piece), piece)
+        kept = mm(act[rows, :], wo[:, out_cols(t)])
+        giv_copy(r).wait_recv()
+        proj = (kept + grecv[r].astype(F32)) * scl[rows, 0:1]
+        blk[z * 2 + c, t, half, strip(q), :] = (res[rows, :].astype(F32) + proj).astype(BF16)
+        c_copy(z, t, half, q).start()
+
+    def on_land(zq, h, half, q):
+        @pl.when((h == 0) & (q == 0))
+        def _():
+            m_copy(2, zq, c, half).wait_recv()
+            m_copy(2, zq, c, half).start()
+
+        arrived(zq, c, side(h), half, q)
+        c_copy(zq, side(h), half, q).start()
+
+    def on_z(way):
+        def send(zq, h, half, q):
+            @pl.when((h == 0) & (q == 0))
+            def _():
+                m_copy(way, zq, c, half).start()
+
+            z_copy(way, zq, h, half, q).start()
+
+        return send
+
+    def on_across(zq, h, half, q):
+        x_copy(zq, half, q).start()
+
+    def on_hidden(zq, h, half, q):
+        m_copy(2, zq, 1 - c, half).wait_recv()
+        for hh in range(2):
+            for qq in range(2):
+                arrived(zq, 1 - c, hh, half, qq)
+        hidden(zq, half)
+        hid_copy(zq, half).start()
+
+        @pl.when(zq == z)
+        def _():
+            shared(half)
+            sh_copy(half).start()
+
+    def on_result(zq, h, half, q):
+        results(zq, half)
+
+    def on_combine(zq, h, half, q):
+        rows = strip(q)
+        sib_copy(zq, half, q).wait_recv()
         end = is_end(zq)
-        for q in range(2):
-            rows = slice(q * piece, (q + 1) * piece)
-
-            @pl.when(end)
-            def _():
-                acc[zq, half, rows, :] = (
-                    acc[zq, half, rows, :].astype(F32) + sib[zq, half, rows, :].astype(F32)
-                ).astype(BF16)
-
-            @pl.when(jnp.logical_not(end))
-            def _():
-                back_copy(zq, half, q, zq, up).wait_recv()
-                acc[zq, half, rows, :] = (
-                    acc[zq, half, rows, :].astype(F32)
-                    + sib[zq, half, rows, :].astype(F32)
-                    + back[zq, half, rows, :].astype(F32)
-                ).astype(BF16)
-
-            @pl.when(zq > z)
-            def _():
-                back_copy(zq, half, q, zq, up).start()
-
-            @pl.when(zq < z - 1)
-            def _():
-                back_copy(zq, half, q, zq, down).start()
-
-            @pl.when(zq == z - 1)
-            def _():
-                back_copy(zq, half, q, n_z, down).start()
-
-    def pass_ahead(zq, half):
-        @pl.when((zq != z) & (half == 0))
+
+        @pl.when(end)
         def _():
-            m_copy(2, zq, c).wait_recv()
-
-            @pl.when((zq < z) & hi)
-            def _():
-                m_copy(0, zq, c).start()
-
-            @pl.when((zq > z) & lo)
-            def _():
-                m_copy(1, zq, c).start()
-
-            m_copy(2, zq, c).start()
-
-        for q in range(2):
-
-            @pl.when(zq != z)
-            def _():
-                arrived(zq, c, t, half, q)
-
-                @pl.when((zq < z) & hi)
+            acc[zq, half, rows, :] = (
+                acc[zq, half, rows, :].astype(F32) + sib[zq, half, rows, :].astype(F32)
+            ).astype(BF16)
+
+        @pl.when(jnp.logical_not(end))
+        def _():
+            back_copy(zq, half, q, zq, up).wait_recv()
+            acc[zq, half, rows, :] = (
+                acc[zq, half, rows, :].astype(F32)
+                + sib[zq, half, rows, :].astype(F32)
+                + back[zq, half, rows, :].astype(F32)
+            ).astype(BF16)
+
+        @pl.when(zq > z)
+        def _():
+            back_copy(zq, half, q, zq, up).start()
+
+        @pl.when(zq < z - 1)
+        def _():
+            back_copy(zq, half, q, zq, down).start()
+
+        @pl.when(zq == z - 1)
+        def _():
+            back_copy(zq, half, q, n_z, down).start()
+
+    actions = (
+        on_stream,
+        on_land,
+        on_z(0),
+        on_z(1),
+        on_across,
+        on_hidden,
+        on_result,
+        on_combine,
+    )
+    order, _ = plan(n_z)
+    groups = max(-(-len(order[zz]) // 3) for zz in range(n_z))
+    tables = [
+        encode(order[zz] + [("combine", zz, 0, 0, 0)] * (3 * groups - len(order[zz])))
+        for zz in range(n_z)
+    ]
+    values = [
+        sum((z == zz).astype(jnp.int32) * tables[zz][g] for zz in range(n_z)) for g in range(groups)
+    ]
+
+    @pl.loop(0, groups)
+    def _(g):
+        value = sum((g == k).astype(jnp.int32) * values[k] for k in range(groups))
+
+        def turn(k, rest):
+            code = rest % 256
+            q, half, h = code % 2, code // 2 % 2, code // 4 % 2
+            zq, kind = code // 8 % 4, code // 32
+            for n, action in enumerate(actions):
+                live = kind == n
+                if action is on_combine:
+                    live = live & (zq != z)
+
+                @pl.when(live)
                 def _():
-                    z_copy(0, zq, half, q).start()
-
-                @pl.when((zq > z) & lo)
-                def _():
-                    z_copy(1, zq, half, q).start()
-
-                c_copy(zq, t, half, q).start()
-
-            x_copy(zq, half, q).start()
-
-        @pl.when((zq == z - 1) & (half == 1) & hi)
-        def _():
-            for q in range(2):
-                z_copy(0, z, 1, q).start()
-
-        @pl.when((zq == z + 1) & (half == 1) & lo)
-        def _():
-            for q in range(2):
-                z_copy(1, z, 1, q).start()
-
-    def pass_across(zq, half):
-        for q in range(2):
-            arrived(zq, c, 1 - t, half, q)
-            c_copy(zq, 1 - t, half, q).start()
-
-    def gathered(zq, half):
-        @pl.when(half == 0)
-        def _():
-            m_copy(2, zq, 1 - c).wait_recv()
-
-        for h in range(2):
-            for q in range(2):
-                arrived(zq, 1 - c, h, half, q)
-
-    def item(code):
-        return (code - 1) // SPLIT, (code - 1) % SPLIT
-
-    tables, base = plan(n_z)
-    codes = []
-    for k in range(len(tables[0])):
-        value = 0
-        for zz in range(n_z):
-            value = value + (z == zz).astype(jnp.int32) * tables[zz][k]
-        codes.append(value)
-
-    def turn(i, carry):
-        now, ahead0, ahead1, close0, close1, prev = carry
-        here = i >= 2
-        cur = jnp.where(here, now % base, 0)
-
-        @pl.when(cur > 0)
-        def _():
-            pass_across(*item(cur))
-
-        @pl.when(prev > 0)
-        def _():
-            results(*item(prev))
-
-        @pl.when(cur > 0)
-        def _():
-            zq, half = item(cur)
-            gathered(zq, half)
-            hidden(zq, half)
-            hid_copy(zq, half).start()
-
-            @pl.when(zq == z)
-            def _():
-                shared(half)
-                sh_copy(half).start()
-
-        @pl.loop(0, 2)
-        def _(k):
-            code = ahead0 % base * (1 - k) + ahead1 % base * k
-
-            @pl.when(code > 0)
-            def _():
-                pass_ahead(*item(code))
-
-        closing = i >= 3
-
-        @pl.when(closing)
-        def _():
-            @pl.loop(0, 2)
-            def _(k):
-                code = close0 % base * (1 - k) + close1 % base * k
-
-                @pl.when(code > 0)
-                def _():
-                    combine(*item(code))
-
-        def shift(value, live):
-            return jnp.where(live, value // base, value)
-
-        return (
-            shift(now, here),
-            ahead0 // base,
-            ahead1 // base,
-            shift(close0, closing),
-            shift(close1, closing),
-            cur,
-        )
-
-    lax.fori_loop(0, n_items + 3, turn, tuple(codes) + (jnp.int32(0),))
+                    action(zq, h, half, q)
+
+            return rest // 256
+
+        lax.fori_loop(0, 3, turn, value)
 
     for half in range(SPLIT):
-        sib_copy(z, half).wait_recv()
         sh_copy(half).wait_recv()
         for q in range(2):
+            sib_copy(z, half, q).wait_recv()
 
             @pl.when(lo)
             def _():
@@ -793,35 +829,48 @@
     for half in range(SPLIT):
         sh_copy(half).wait_send()
 
+    def listed(target, half, q):
+        inner = (target > 0) & (target < n_z - 1)
+        outer_in, inner_in = half * 2 + q in FULL[0], half * 2 + q in FULL[1]
+        return (inner & inner_in) | (jnp.logical_not(inner) & outer_in)
+
+    for half in range(SPLIT):
+        for q in range(2):
+            for way, there, target in ((0, hi, z + 1), (1, lo, z - 1)):
+
+                @pl.when(there & listed(target, half, q))
+                def _():
+                    z_copy(way, z, 1, half, q).wait_send()
+
     @pl.loop(0, n_z)
     def _(zq):
-        @pl.when(hi & (zq <= z))
-        def _():
-            m_copy(0, zq, c).wait_send()
-            for half in range(SPLIT):
-                for q in range(2):
-                    z_copy(0, zq, half, q).wait_send()
-
-        @pl.when(lo & (zq >= z))
-        def _():
-            m_copy(1, zq, c).wait_send()
-            for half in range(SPLIT):
-                for q in range(2):
-                    z_copy(1, zq, half, q).wait_send()
-
-        m_copy(2, zq, c).wait_send()
+        for way, there in ((0, hi & (zq <= z)), (1, lo & (zq >= z))):
+
+            @pl.when(there)
+            def _():
+                for half in range(SPLIT):
+                    m_copy(way, zq, c, half).wait_send()
+                    for q in range(2):
+                        z_copy(way, zq, 0, half, q).wait_send()
+
+        near = (zq == z + 1) | (zq == z - 1)
         for half in range(SPLIT):
+            m_copy(2, zq, c, half).wait_send()
             for q in range(2):
-                x_copy(zq, half, q).wait_send()
+
+                @pl.when(jnp.logical_not(near & listed(z, half, q)))
+                def _():
+                    x_copy(zq, half, q).wait_send()
+
                 for h in range(2):
                     c_copy(zq, h, half, q).wait_send()
+                sib_copy(zq, half, q).wait_send()
 
                 @pl.when(zq != z)
                 def _():
                     back_copy(zq, half, q, zq, up).wait_send()
 
             hid_copy(zq, half).wait_send()
-            sib_copy(zq, half).wait_send()
 
 
 def fast(
@@ -851,11 +900,6 @@
     experts = n_sp * EXP_DEV
     most = max(1, 2 * rows * TOPK // experts)
     lanes = 128
-    docs = jnp.broadcast_to(doc_ids.astype(F32)[:, None], (tokens, lanes))
-    info = jnp.concatenate([routing.astype(F32), route_weight], axis=1)
-    info = info.reshape(SPLIT, rows, 2 * TOPK).transpose(0, 2, 1)
-    info = jnp.pad(info, ((0, 0), (0, 8 - 2 * TOPK), (0, -rows % lanes)), constant_values=-1.0)
-
     piece = rows // 2
     blocks = n_sp
     unit = expert_gate.shape[2]
@@ -865,7 +909,7 @@
     return pl.pallas_call(
         functools.partial(layer_kernel, n_z, most),
         out_shape=jax.ShapeDtypeStruct((tokens, cols), BF16),
-        in_specs=[hbm] * 5 + [vm] * 5 + [hbm] * 6,
+        in_specs=[hbm] * 5 + [vm] * 6 + [hbm] * 6,
         out_specs=vm,
         scratch_shapes=[
             pltpu.VMEM((tokens, chan), BF16),
@@ -892,7 +936,7 @@
             pltpu.VMEM((2, 8, cols), F32),
             pltpu.VMEM((rows, rows), BF16),
             pltpu.VMEM((blocks, 2, SPLIT, rows, cols), BF16),
-            pltpu.VMEM((blocks,) + info.shape, F32),
+            pltpu.VMEM((blocks, SPLIT, 8, rows + -rows % lanes), F32),
             pltpu.VMEM((EXP_DEV, 2 * most, width), BF16),
             pltpu.VMEM((2, n_z, SPLIT, EXP_DEV, 2 * most, unit), BF16),
             pltpu.VMEM((2, SPLIT, rows, unit), BF16),
@@ -907,18 +951,18 @@
             dma((2,)),
             dma((2 * SPLIT,)),
             dma((2 * SPLIT,)),
-            dma((2, n_z, SPLIT, 2)),
+            dma((2, n_z + 1, SPLIT, 2)),
             dma((n_z, SPLIT, 2)),
             dma((n_z, 2, SPLIT, 2)),
             dma((blocks, 2, SPLIT, 2)),
-            dma((3, n_z)),
-            dma((blocks,)),
+            dma((3, n_z, SPLIT)),
+            dma((blocks, SPLIT)),
             dma((n_z, SPLIT)),
             dma((n_z, SPLIT)),
             dma((SPLIT,)),
             dma((SPLIT,)),
-            dma((n_z, SPLIT)),
-            dma((n_z, SPLIT)),
+            dma((n_z, SPLIT, 2)),
+            dma((n_z, SPLIT, 2)),
             dma((n_z, SPLIT, 2)),
             dma((n_z + 1, SPLIT, 2)),
         ],
@@ -931,11 +975,12 @@
         conv_input,
         residual,
         out_weight,
-        docs,
+        doc_ids[None, :],
         conv_taps,
         mix_gain[None, :],
         ffn_gain[None, :],
-        info,
+        routing.T,
+        route_weight.T,
         expert_gate,
         expert_up,
         expert_down,

time: 136 us -> 120 us (0.88)
  the two profiles are of different devices: /device:TPU:13 before, /device:TPU:0 now
where the time goes in v2:
time: 120 us
  Pallas kernels  117 us (98%)
  local copies, waits for them, and re-layouts  3.31 us (3%)
    pallas_call x1, Pallas kernels, fast(): pl.pallas_call(functools.partial(layer_kernel, n_z, most), out_shape=jax....  117 us

profile of v2, /device:TPU:0, one launch (start us, length us, event | category | flops | bytes accessed | tf_op | source)
XLA Modules:
  0.0 120.1 jit_solution(16148444147297133181)
XLA Ops:
  0.0 1.2 %broadcast_in_dim.9.docs_ref = s32[1,384]{1,0:T(1,128)} reshape(s32[384]{0:T(512)} %param.20) | data formatting | bytes 3072 | tf_op jit(solution)/shard_map/broadcast_in_dim | solution.py:978
  1.2 116.8 %shard_map.163 = bf16[384,1024]{1,0:T(8,128)(2,1)} custom-call(bf16[384,512]{1,0:T(8,128)(2,1)} %og_hbm.1, bf16[384,512]{1,0:T(8,128)(2,1)} %ig_hbm.1, bf16[384,512]{1,0:T(8,128)(2,1)} %ci_hbm.1, bf16[384,1024]{1,0:T(8,128)(2,1)} %res_hbm.1, bf16[512,2048]{1,0:T(8,128)(2,1)} %wo_hbm.1, s32[1,384]{1,0:T(1,128)} %broadcast_in_dim.9.docs_ref, ...), custom_call_target="tpu_custom_call" | custom-call | tf_op jit(solution)/shard_map/pallas_call | solution.py:909
  118.1 2.1 %copy.19 = bf16[384,1024]{1,0:T(8,128)(2,1)} copy(bf16[384,1024]{1,0:T(8,128)(2,1)} %shard_map.163) | data formatting | bytes 1572864

commit v3 on v2

--- a/solution.py
+++ b/solution.py
@@ -138,9 +138,19 @@
 SPLIT = 2
 
 
+GIVEN = (1, 0, 2, 3)
+HOP, START, WIRE, NEAR = 2.8, 4.5, 4.18, (1.4, 2.5)
+COST, EXTRA = (0.45, 0.15, 0.15, 0.15, 0.15, 1.65, 1.3, 0.22), (0.9, 0.3)
 FULL = ((0, 1), (0, 1))
-HOP, START, DEPTH = 2.8, 6.0, 1.0
-W = (8.4, 6.0, 3.8, -3.3, 5.9, 4.9, 4.7, -4.7, -0.8, 1.6, 5.9, 3.4, 5.6)
+ROWX = (4.4, 6.8, -4.4, 5.1, -5, 1.7, -0.6, -5.3)
+ROWZ = (3.5, 5.9, -6, 3.6, -2.6, 0, -1.7, -4.6)
+ROWF = (-5.4, -6.7)
+COMB = (-3.8, -2, 3, -5.8, -4.1, 0.2, -0.3, 1)
+WORK = (4.9, 1.9, 4.4, 2.3, 5, -3.8, 6.2, -1.2)
+RANK, DEPTH = (0, 0, 1, 4, 0), (1, 1.5)
+BASE = 257
+
+
 KINDS = ("stream", "land", "up", "down", "across", "hidden", "result", "combine")
 
 
@@ -149,18 +159,15 @@
 
 
 def plan(n_z):
-    wire, hop, near = 4.2, HOP, 1.6
-    cost = dict(
-        stream=0.35, land=0.1, up=0.1, down=0.1, across=0.1, hidden=1.7, result=1.35, combine=0.3
-    )
     chunks = [(half, q) for half in range(SPLIT) for q in range(2)]
     zones = range(n_z)
-    have, told, heard, summed, went = {}, {}, {}, {}, {}
+    never = 1e9
+    have, told, heard, summed, went, final, arrive = {}, {}, {}, {}, {}, {}, {}
     todo = {z: [] for z in zones}
     for z in zones:
         for k, (half, q) in enumerate(chunks):
             todo[z].append(("stream", z, 0, half, q))
-            went[z, z, half, q] = START + wire * (k + 1) + hop
+            went[z, half, q] = START + WIRE * (GIVEN.index(k) + 1) + HOP
         for zq in zones:
             for half, q in chunks:
                 if zq != z:
@@ -172,56 +179,61 @@
                     todo[z].append(("down", zq, 0, half, q))
                 if not full_rows(n_z, zq, z, half, q):
                     todo[z].append(("across", zq, 0, half, q))
+                todo[z].append(("combine", zq, 0, half, q))
             for half in range(SPLIT):
                 todo[z].append(("hidden", zq, 0, half, 0))
                 todo[z].append(("result", zq, 0, half, 0))
-                if zq != z:
-                    todo[z] += [("combine", zq, 0, half, q) for q in range(2)]
         for half, q in chunks:
             if z < n_z - 1 and full_rows(n_z, z, z + 1, half, q):
                 todo[z].append(("up", z, 1, half, q))
             if z > 0 and full_rows(n_z, z, z - 1, half, q):
                 todo[z].append(("down", z, 1, half, q))
-    arrive = {}
     link = {(z, way): 0.0 for z in zones for way in ("up", "down", "across")}
     for z in zones:
-        link[z, "across"] = START + wire * len(chunks)
-    core = {z: 0.0 for z in zones}
-    never = 1e9
+        link[z, "across"] = START + WIRE * len(chunks)
+    core = {z: START for z in zones}
 
     def put(z, way, now, size):
-        begin = max(now, link[z, way])
-        link[z, way] = begin + wire * size
-        return link[z, way] + hop
+        link[z, way] = max(now, link[z, way]) + WIRE * size
+        return link[z, way] + HOP
 
     def ready(z, event):
         kind, zq, h, half, q = event
         if kind == "stream":
-            return went[z, z, half, q]
+            return went[z, half, q]
         if kind == "land":
             return arrive.get((z, zq, h, half, q), never)
         if kind in ("up", "down", "across"):
-            return max(have.get((z, zq, h, half, q), never), link[z, kind] - DEPTH)
+            depth = DEPTH[kind == "across"]
+            return max(have.get((z, zq, h, half, q), never), link[z, kind] - depth)
         if kind == "hidden":
-            return max(have.get((z, zq, g, half, p), never) for g in range(2) for p in range(2)) + near
+            parts = [have.get((z, zq, g, half, p), never) for g in range(2) for p in range(2)]
+            return max(parts) + NEAR[0]
         if kind == "result":
             return heard.get((z, zq, half), never)
-        before = z - 1 if zq > z else z + 1
-        coming = summed.get((before, zq, half, q), never) if 0 <= before < n_z else 0.0
-        return max(told.get((z, zq, half), never), coming)
+        at = told.get((z, zq, half), never)
+        if zq >= z and z > 0:
+            at = max(at, summed.get((z - 1, zq, half, q), never))
+        if zq <= z and z < n_z - 1:
+            at = max(at, summed.get((z + 1, zq, half, q), never))
+        if zq == z and q > 0:
+            at = max(at, final.get((z, half, q - 1), never))
+        return at
 
     def rank(z, event):
         kind, zq, h, half, q = event
         away = abs(zq - z)
         if kind in ("stream", "land"):
-            return (0, 0.0)
+            return (RANK[0], 0.0, q)
         if kind == "combine":
-            return (1, W[12] * away + half)
-        if kind in ("result", "hidden"):
-            return (2, (kind == "hidden") * 1.0, W[11] * away)
+            return (RANK[1], COMB[away * 2 + half], q)
+        if kind == "result":
+            return (RANK[2], WORK[away * 2 + half], q)
+        if kind == "hidden":
+            return (RANK[3], WORK[away * 2 + half], q)
         if kind == "across":
-            return (3, W[away] + W[4] * half, q)
-        return (3, (W[9] if h else W[5 + away]) + W[10] * half, q)
+            return (RANK[4], ROWX[away * 2 + half], q)
+        return (RANK[4], ROWZ[away * 2 + half] if h == 0 else ROWF[half], q)
 
     order = {z: [] for z in zones}
     while any(todo.values()):
@@ -239,33 +251,34 @@
         kind, zq, h, half, q = event
         todo[z].remove(event)
         order[z].append(event)
-        end = at + cost[kind] + (0.9 if kind == "hidden" and zq == z else 0.0)
+        end = at + COST[KINDS.index(kind)]
+        if zq == z:
+            end = end + (EXTRA[0] if kind == "hidden" else EXTRA[1] if kind == "combine" else 0.0)
         core[z] = end
         if kind in ("stream", "land"):
             have[z, zq, h, half, q] = end
         elif kind in ("up", "down"):
-            arrive[z + (1 if kind == "up" else -1), zq, h, half, q] = put(z, kind, end, 1)
+            arrive[z + (1 if kind == "up" else -1), zq, h, half, q] = put(z, kind, end, 1.0)
         elif kind == "across":
-            arrive[z, zq, 1, half, q] = put(z, kind, end, 1)
+            arrive[z, zq, 1, half, q] = put(z, kind, end, 1.0)
         elif kind == "hidden":
             heard[z, zq, half] = put(z, "across", end, 1.0 if zq == z else 0.5)
         elif kind == "result":
-            told[z, zq, half] = end + 2.2
+            told[z, zq, half] = end + NEAR[1]
+        elif zq == z:
+            final[z, half, q] = end
         else:
-            summed[z, zq, half, q] = put(z, "up" if zq > z else "down", end, 1)
-    done = max(max(core.values()), max(summed.values()))
-    return order, done
-
-
-def encode(events):
+            summed[z, zq, half, q] = put(z, "up" if zq > z else "down", end, 1.0)
+    return order, max(final.values())
+
+
+def encode(events, slots):
     codes = [
-        (((KINDS.index(kind) * 4 + zq) * 2 + h) * 2 + half) * 2 + q
+        (((KINDS.index(kind) * 4 + zq) * 2 + h) * 2 + half) * 2 + q + 1
         for kind, zq, h, half, q in events
     ]
-    return [
-        sum(code << (8 * k) for k, code in enumerate(codes[at : at + 3]))
-        for at in range(0, len(codes), 3)
-    ]
+    codes += [0] * (slots - len(codes))
+    return [sum(codes[at + k] * BASE**k for k in range(3)) for at in range(0, slots, 3)]
 
 
 def layer_kernel(
@@ -288,7 +301,7 @@
     sg_hbm,
     su_hbm,
     sd_hbm,
-    out_ref,
+    out_hbm,
     og,
     ig,
     ci,
@@ -307,7 +320,6 @@
     act,
     ssq,
     srow,
-    scl,
     gsend,
     grecv,
     fg,
@@ -322,6 +334,7 @@
     outgo,
     sib,
     back,
+    done,
     load_sem,
     halo_sem,
     sum_sem,
@@ -342,6 +355,7 @@
     sib_recv,
     back_send,
     back_recv,
+    out_sem,
 ):
     first = [
         pltpu.make_async_copy(src, dst, load_sem.at[n])
@@ -362,7 +376,7 @@
     z = s // 2
     c = s % 2
     tokens, chan = ig.shape
-    cols = out_ref.shape[1]
+    cols = res.shape[1]
     width = 2 * cols
     half_rows = tokens // SPLIT
     piece = half_rows // 2
@@ -453,8 +467,8 @@
     def halo_copy():
         return remote(hsend, hrecv, halo_sem.at[0], halo_sem.at[1], after)
 
-    def sum_copy():
-        return remote(srow.at[0], srow.at[1], sum_sem.at[0], sum_sem.at[1], peer)
+    def sum_copy(r):
+        return remote(srow.at[0, r], srow.at[1, r], sum_sem.at[0, r], sum_sem.at[1, r], peer)
 
     def fg_copy():
         return remote(fg.at[t], fg.at[t], fg_sem.at[0], fg_sem.at[1], peer)
@@ -507,7 +521,70 @@
         meta[own, half] = jnp.zeros(meta.shape[2:], F32)
         meta[own, half, 0:TOPK, :half_rows] = names[:, part]
         meta[own, half, TOPK : 2 * TOPK, :half_rows] = share[:, part]
-    fg[t] = jnp.broadcast_to(ffn_ref[...], fg.shape[1:])
+    fg[t] = ffn_ref[...]
+    step_rows = 32
+
+    @pl.loop(0, tokens // step_rows)
+    def _(i):
+        at = pl.multiple_of(i * step_rows, step_rows)
+        ext[pl.ds(pad + at, step_rows), :] = product(pl.ds(at, step_rows))
+
+    n_tri = tri.shape[0]
+    row_id = lax.broadcasted_iota(jnp.int32, (n_tri, n_tri), 0)
+    col_id = lax.broadcasted_iota(jnp.int32, (n_tri, n_tri), 1)
+    tri[...] = (row_id < col_id).astype(F32).astype(BF16)
+
+    def convolve(r):
+        @pl.loop(0, piece // step_rows)
+        def _(i):
+            at = pl.multiple_of(r * piece + i * step_rows, step_rows)
+            v = ext[pl.ds(pl.multiple_of(pad - 8 + at, 8), step_rows + 8), :]
+            d = dext[pl.ds(pl.multiple_of(pad - 8 + at, 8), step_rows + 8), :]
+            doc = d[8:]
+            mixed = None
+            for k in range(CONV_K):
+                by = CONV_K - 1 - k
+                if by:
+                    same = (pltpu.roll(d, by, 0)[8:] == doc).astype(F32)
+                    same = jnp.concatenate([same] * (chan // lanes), axis=1)
+                    term = taps_ref[k : k + 1, :] * pltpu.roll(v, by, 0)[8:] * same
+                else:
+                    term = taps_ref[k : k + 1, :] * v[8:]
+                mixed = term if mixed is None else mixed + term
+            rows = pl.ds(at, step_rows)
+            conv_out = og[rows, :].astype(F32) * mixed
+            total = jnp.sum(conv_out * conv_out, axis=1, keepdims=True)
+            ssq[rows, :] = jnp.broadcast_to(total, (step_rows, lanes))
+            act[rows, :] = (conv_out * mix_ref[...]).astype(BF16)
+
+    n_chunks = 2 * SPLIT
+    eye_piece = lax.broadcasted_iota(jnp.int32, (piece, lanes), 0) == lax.broadcasted_iota(
+        jnp.int32, (piece, lanes), 1
+    )
+
+    def out_cols(who):
+        return pl.ds(pl.multiple_of(who * cols, cols), cols)
+
+    def sums(r):
+        part = ssq[r * piece : (r + 1) * piece, :]
+        line = jnp.sum(jnp.where(eye_piece, part, F32(0.0)), axis=0, keepdims=True)
+        srow[0, r] = jnp.broadcast_to(line, srow.shape[2:])
+
+    def give(r):
+        gsend[r] = mm(act[r * piece : (r + 1) * piece, :], wo[:, out_cols(1 - t)]).astype(BF16)
+
+    def send_given(r):
+        sum_copy(r).start()
+        giv_copy(r).start()
+
+    first[2].wait()
+    for r in GIVEN:
+        if r:
+            convolve(r)
+            sums(r)
+    first[3].wait()
+    give(GIVEN[0])
+    first[4].wait()
     arrivals = (
         2
         + lo.astype(jnp.int32)
@@ -522,24 +599,9 @@
         halo_copy().start()
 
     fg_copy().start()
+    send_given(GIVEN[0])
     for half in range(SPLIT):
         m_copy(2, z, c, half).start()
-
-    step_rows = 32
-
-    @pl.loop(0, tokens // step_rows)
-    def _(i):
-        at = pl.multiple_of(i * step_rows, step_rows)
-        ext[pl.ds(pad + at, step_rows), :] = product(pl.ds(at, step_rows))
-
-    n_tri = tri.shape[0]
-    row_id = lax.broadcasted_iota(jnp.int32, (n_tri, n_tri), 0)
-    col_id = lax.broadcasted_iota(jnp.int32, (n_tri, n_tri), 1)
-    tri[...] = (row_id < col_id).astype(F32).astype(BF16)
-    for load in first[2:]:
-        load.wait()
-    for load in later:
-        load.start()
 
     @pl.when(has_prev)
     def _():
@@ -550,54 +612,14 @@
     @pl.when(jnp.logical_not(has_prev))
     def _():
         ext[pad - 8 : pad, :] = jnp.zeros((8, chan), F32)
-        dext[pad - 8 : pad, :] = jnp.zeros((8, dext.shape[1]), F32)
-
-    @pl.loop(0, tokens // step_rows)
-    def _(i):
-        at = pl.multiple_of(i * step_rows, step_rows)
-        v = ext[pl.ds(pl.multiple_of(pad - 8 + at, 8), step_rows + 8), :]
-        d = dext[pl.ds(pl.multiple_of(pad - 8 + at, 8), step_rows + 8), :]
-        doc = d[8:]
-        mixed = None
-        for k in range(CONV_K):
-            by = CONV_K - 1 - k
-            if by:
-                same = (pltpu.roll(d, by, 0)[8:] == doc).astype(F32)
-                same = jnp.concatenate([same] * (chan // lanes), axis=1)
-                term = taps_ref[k : k + 1, :] * pltpu.roll(v, by, 0)[8:] * same
-            else:
-                term = taps_ref[k : k + 1, :] * v[8:]
-            mixed = term if mixed is None else mixed + term
-        rows = pl.ds(at, step_rows)
-        conv_out = og[rows, :].astype(F32) * mixed
-        total = jnp.sum(conv_out * conv_out, axis=1, keepdims=True)
-        ssq[rows, :] = jnp.broadcast_to(total, (step_rows, lanes))
-        act[rows, :] = (conv_out * mix_ref[...]).astype(BF16)
-
-    for k in range(tokens // lanes):
-        part = ssq[k * lanes : (k + 1) * lanes, :]
-        line = jnp.sum(jnp.where(eye, part, F32(0.0)), axis=0, keepdims=True)
-        srow[0, :, k * lanes : (k + 1) * lanes] = jnp.broadcast_to(line, (8, lanes))
-    sum_copy().start()
-
-    n_chunks = 2 * SPLIT
-
-    def out_cols(who):
-        return pl.ds(pl.multiple_of(who * cols, cols), cols)
-
-    for r in range(n_chunks):
-        gsend[r] = mm(act[r * piece : (r + 1) * piece, :], wo[:, out_cols(1 - t)]).astype(BF16)
-        giv_copy(r).start()
-
-    sum_copy().wait_recv()
-    for k in range(tokens // lanes):
-        line = srow[1, 0:1, k * lanes : (k + 1) * lanes]
-        whole = ssq[k * lanes : (k + 1) * lanes, :] + upright(line)
-        scl[k * lanes : (k + 1) * lanes, :] = lax.rsqrt(whole / (2 * chan) + 1e-06)
-
+        dext[pad - 8 : pad, :] = jnp.zeros((8, lanes), F32)
+
+    convolve(0)
+    sums(0)
+    for r in GIVEN[1:]:
+        give(r)
+        send_given(r)
     fg_copy().wait_recv()
-    for load in later:
-        load.wait()
 
     def picks(zq, cq, half):
         info = meta[zq * 2 + cq, half][:, :half_rows]
@@ -676,10 +698,24 @@
         r = half * 2 + q
         rows = pl.ds(pl.multiple_of(r * piece, piece), piece)
         kept = mm(act[rows, :], wo[:, out_cols(t)])
+        sum_copy(r).wait_recv()
+        line = srow[1, r, 0:1, :]
+        theirs = jnp.sum(jnp.where(eye_piece, line, F32(0.0)), axis=1, keepdims=True)
+        scale = lax.rsqrt((ssq[rows, 0:1] + theirs) / (2 * chan) + 1e-06)
         giv_copy(r).wait_recv()
-        proj = (kept + grecv[r].astype(F32)) * scl[rows, 0:1]
+        proj = (kept + grecv[r].astype(F32)) * scale
         blk[z * 2 + c, t, half, strip(q), :] = (res[rows, :].astype(F32) + proj).astype(BF16)
         c_copy(z, t, half, q).start()
+
+        @pl.when(r == GIVEN[0])
+        def _():
+            for load in later:
+                load.start()
+
+        @pl.when(r == GIVEN[-1])
+        def _():
+            for load in later:
+                load.wait()
 
     def on_land(zq, h, half, q):
         @pl.when((h == 0) & (q == 0))
@@ -719,37 +755,77 @@
     def on_result(zq, h, half, q):
         results(zq, half)
 
+    def out_copy(half, q):
+        return pltpu.make_async_copy(
+            done.at[half, pl.ds(q * piece, piece)],
+            out_hbm.at[pl.ds(half * half_rows + q * piece, piece)],
+            out_sem.at[half, q],
+        )
+
+    def finish(half, q):
+        rows = strip(q)
+
+        @pl.when(q == 0)
+        def _():
+            sh_copy(half).wait_recv()
+
+        fin = (
+            blk[z * 2 + c, t, half, rows, :].astype(F32)
+            + mm(shid[0, half, rows, :], sd[:unit, :])
+            + mm(shid[1, half, rows, :], sd[unit:, :])
+            + acc[z, half, rows, :].astype(F32)
+            + sib[z, half, rows, :].astype(F32)
+        )
+
+        @pl.when(lo)
+        def _():
+            back_copy(z, half, q, z, up).wait_recv()
+
+        @pl.when(hi)
+        def _():
+            back_copy(z, half, q, n_z, up).wait_recv()
+
+        low = jnp.where(lo, back[z, half, rows, :].astype(F32), F32(0.0))
+        high = jnp.where(hi, back[n_z, half, rows, :].astype(F32), F32(0.0))
+        done[half, rows, :] = (fin + low + high).astype(BF16)
+        out_copy(half, q).start()
+
     def on_combine(zq, h, half, q):
         rows = strip(q)
         sib_copy(zq, half, q).wait_recv()
-        end = is_end(zq)
-
-        @pl.when(end)
+
+        @pl.when(zq == z)
         def _():
-            acc[zq, half, rows, :] = (
-                acc[zq, half, rows, :].astype(F32) + sib[zq, half, rows, :].astype(F32)
-            ).astype(BF16)
-
-        @pl.when(jnp.logical_not(end))
+            finish(half, q)
+
+        @pl.when(zq != z)
         def _():
-            back_copy(zq, half, q, zq, up).wait_recv()
-            acc[zq, half, rows, :] = (
-                acc[zq, half, rows, :].astype(F32)
-                + sib[zq, half, rows, :].astype(F32)
-                + back[zq, half, rows, :].astype(F32)
-            ).astype(BF16)
-
-        @pl.when(zq > z)
-        def _():
-            back_copy(zq, half, q, zq, up).start()
-
-        @pl.when(zq < z - 1)
-        def _():
-            back_copy(zq, half, q, zq, down).start()
-
-        @pl.when(zq == z - 1)
-        def _():
-            back_copy(zq, half, q, n_z, down).start()
+            @pl.when(is_end(zq))
+            def _():
+                acc[zq, half, rows, :] = (
+                    acc[zq, half, rows, :].astype(F32) + sib[zq, half, rows, :].astype(F32)
+                ).astype(BF16)
+
+            @pl.when(jnp.logical_not(is_end(zq)))
+            def _():
+                back_copy(zq, half, q, zq, up).wait_recv()
+                acc[zq, half, rows, :] = (
+                    acc[zq, half, rows, :].astype(F32)
+                    + sib[zq, half, rows, :].astype(F32)
+                    + back[zq, half, rows, :].astype(F32)
+                ).astype(BF16)
+
+            @pl.when(zq > z)
+            def _():
+                back_copy(zq, half, q, zq, up).start()
+
+            @pl.when(zq < z - 1)
+            def _():
+                back_copy(zq, half, q, zq, down).start()
+
+            @pl.when(zq == z - 1)
+            def _():
+                back_copy(zq, half, q, n_z, down).start()
 
     actions = (
         on_stream,
@@ -763,10 +839,7 @@
     )
     order, _ = plan(n_z)
     groups = max(-(-len(order[zz]) // 3) for zz in range(n_z))
-    tables = [
-        encode(order[zz] + [("combine", zz, 0, 0, 0)] * (3 * groups - len(order[zz])))
-        for zz in range(n_z)
-    ]
+    tables = [encode(order[zz], 3 * groups) for zz in range(n_z)]
     values = [
         sum((z == zz).astype(jnp.int32) * tables[zz][g] for zz in range(n_z)) for g in range(groups)
     ]
@@ -776,58 +849,32 @@
         value = sum((g == k).astype(jnp.int32) * values[k] for k in range(groups))
 
         def turn(k, rest):
-            code = rest % 256
-            q, half, h = code % 2, code // 2 % 2, code // 4 % 2
-            zq, kind = code // 8 % 4, code // 32
+            mark = rest % BASE + 31
+            q, half, h = mark % 2, mark // 2 % 2, mark // 4 % 2
+            zq, kind = mark // 8 % 4, mark // 32
             for n, action in enumerate(actions):
-                live = kind == n
-                if action is on_combine:
-                    live = live & (zq != z)
-
-                @pl.when(live)
+                @pl.when(kind == n + 1)
                 def _():
                     action(zq, h, half, q)
 
-            return rest // 256
+            return rest // BASE
 
         lax.fori_loop(0, 3, turn, value)
-
-    for half in range(SPLIT):
-        sh_copy(half).wait_recv()
-        for q in range(2):
-            sib_copy(z, half, q).wait_recv()
-
-            @pl.when(lo)
-            def _():
-                back_copy(z, half, q, z, up).wait_recv()
-
-            @pl.when(hi)
-            def _():
-                back_copy(z, half, q, n_z, up).wait_recv()
-
-            rows = slice(q * piece, (q + 1) * piece)
-            fin = (
-                blk[z * 2 + c, t, half, rows, :].astype(F32)
-                + mm(shid[0, half, rows, :], sd[:unit, :])
-                + mm(shid[1, half, rows, :], sd[unit:, :])
-                + acc[z, half, rows, :].astype(F32)
-                + sib[z, half, rows, :].astype(F32)
-            )
-            low = jnp.where(lo, back[z, half, rows, :].astype(F32), F32(0.0))
-            high = jnp.where(hi, back[n_z, half, rows, :].astype(F32), F32(0.0))
-            at = half * half_rows + q * piece
-            out_ref[at : at + piece, :] = (fin + low + high).astype(BF16)
 
     @pl.when(has_next)
     def _():
         halo_copy().wait_send()
 
     fg_copy().wait_send()
-    sum_copy().wait_send()
     for r in range(n_chunks):
+        sum_copy(r).wait_send()
         giv_copy(r).wait_send()
     for half in range(SPLIT):
         sh_copy(half).wait_send()
+
+    for half in range(SPLIT):
+        for q in range(2):
+            out_copy(half, q).wait()
 
     def listed(target, half, q):
         inner = (target > 0) & (target < n_z - 1)
@@ -910,7 +957,7 @@
         functools.partial(layer_kernel, n_z, most),
         out_shape=jax.ShapeDtypeStruct((tokens, cols), BF16),
         in_specs=[hbm] * 5 + [vm] * 6 + [hbm] * 6,
-        out_specs=vm,
+        out_specs=hbm,
         scratch_shapes=[
             pltpu.VMEM((tokens, chan), BF16),
             pltpu.VMEM((tokens, chan), BF16),
@@ -929,11 +976,10 @@
             pltpu.VMEM((8, chan + lanes), F32),
             pltpu.VMEM((tokens, chan), BF16),
             pltpu.VMEM((tokens, lanes), F32),
-            pltpu.VMEM((2, 8, tokens), F32),
-            pltpu.VMEM((tokens, lanes), F32),
+            pltpu.VMEM((2, 2 * SPLIT, 8, lanes), F32),
             pltpu.VMEM((2 * SPLIT, piece, cols), BF16),
             pltpu.VMEM((2 * SPLIT, piece, cols), BF16),
-            pltpu.VMEM((2, 8, cols), F32),
+            pltpu.VMEM((2, 1, cols), F32),
             pltpu.VMEM((rows, rows), BF16),
             pltpu.VMEM((blocks, 2, SPLIT, rows, cols), BF16),
             pltpu.VMEM((blocks, SPLIT, 8, rows + -rows % lanes), F32),
@@ -945,9 +991,10 @@
             pltpu.VMEM((n_z, SPLIT, rows, cols), BF16),
             pltpu.VMEM((n_z, SPLIT, rows, cols), BF16),
             pltpu.VMEM((n_z + 1, SPLIT, rows, cols), BF16),
+            pltpu.VMEM((SPLIT, rows, cols), BF16),
             dma((11,)),
             dma((2,)),
-            dma((2,)),
+            dma((2, 2 * SPLIT)),
             dma((2,)),
             dma((2 * SPLIT,)),
             dma((2 * SPLIT,)),
@@ -965,6 +1012,7 @@
             dma((n_z, SPLIT, 2)),
             dma((n_z, SPLIT, 2)),
             dma((n_z + 1, SPLIT, 2)),
+            dma((SPLIT, 2)),
         ],
         compiler_params=pltpu.CompilerParams(
             collective_id=0, has_side_effects=True, vmem_limit_bytes=64 * 1024 * 1024 - 65536

time: 120 us -> 120 us (level)
  no operation moved by 1% of the time
where the time goes in v3:
time: 120 us; the launch traced here: 119 us
  Pallas kernels  116 us (97%)
  local copies, waits for them, and re-layouts  3.31 us (3%)
    pallas_call x1, Pallas kernels, fast(): pl.pallas_call(functools.partial(layer_kernel, n_z, most), out_shape=jax....  116 us

profile of v3, /device:TPU:0, one launch (start us, length us, event | category | flops | bytes accessed | tf_op | source)
XLA Modules:
  0.0 119.4 jit_solution(3845338260907037080)
XLA Ops:
  0.0 1.2 %broadcast_in_dim.9.docs_ref = s32[1,384]{1,0:T(1,128)} reshape(s32[384]{0:T(512)} %param.20) | data formatting | bytes 3072 | tf_op jit(solution)/shard_map/broadcast_in_dim | solution.py:1026
  1.2 116.0 %shard_map.163 = bf16[384,1024]{1,0:T(8,128)(2,1)} custom-call(bf16[384,512]{1,0:T(8,128)(2,1)} %og_hbm.1, bf16[384,512]{1,0:T(8,128)(2,1)} %ig_hbm.1, bf16[384,512]{1,0:T(8,128)(2,1)} %ci_hbm.1, bf16[384,1024]{1,0:T(8,128)(2,1)} %res_hbm.1, bf16[512,2048]{1,0:T(8,128)(2,1)} %wo_hbm.1, s32[1,384]{1,0:T(1,128)} %broadcast_in_dim.9.docs_ref, ...), custom_call_target="tpu_custom_call" | custom-call | tf_op jit(solution)/shard_map/pallas_call | solution.py:956
  117.3 2.1 %copy.19 = bf16[384,1024]{1,0:T(8,128)(2,1)} copy(bf16[384,1024]{1,0:T(8,128)(2,1)} %shard_map.163) | data formatting | bytes 1572864

commit v4 on v3

--- a/solution.py
+++ b/solution.py
@@ -141,21 +141,27 @@
 GIVEN = (1, 0, 2, 3)
 HOP, START, WIRE, NEAR = 2.8, 4.5, 4.18, (1.4, 2.5)
 COST, EXTRA = (0.45, 0.15, 0.15, 0.15, 0.15, 1.65, 1.3, 0.22), (0.9, 0.3)
-FULL = ((0, 1), (0, 1))
-ROWX = (4.4, 6.8, -4.4, 5.1, -5, 1.7, -0.6, -5.3)
-ROWZ = (3.5, 5.9, -6, 3.6, -2.6, 0, -1.7, -4.6)
-ROWF = (-5.4, -6.7)
-COMB = (-3.8, -2, 3, -5.8, -4.1, 0.2, -0.3, 1)
-WORK = (4.9, 1.9, 4.4, 2.3, 5, -3.8, 6.2, -1.2)
-RANK, DEPTH = (0, 0, 1, 4, 0), (1, 1.5)
+FULL = ((0, 2, 3), (0,), (1, 2, 3))
+ROWX = (3.2, 7.8, -0.1, 7, 2.4, 1.9, -0.8, -4.5, -6.9, -1.3, -4.6, -1.2, -3.6, -2.7, -3.5, -1.3)
+ROWZ = (5.3, -4.7, 3.6, 4.1, 6.5, 4, 5.6, -2.5, -3.8, 5.1, 3.9, -2.9, -5.3, 4.7, -3.6, 0.2)
+ROWF = (-0.1, -5.8, 4.7, 4.9)
+COMB = (5, -4.9, -3.1, 0.6, -2, -2.4, 5.5, -0.2, -1.5, -3.6, -4.8, 1.4, -0.4, 7.5, -2.3, -2.3)
+WORK = (-3.4, 3.1, -3.1, 1.5, 1.1, -1.8, 5.4, -5.7, -0.1, 1.1, -4, 2.1, -4.3, 1.7, -0.5, 1)
+RANK = (4, 0, 0, 0, 4)
+DEPTH = (1, 2)
 BASE = 257
 
 
 KINDS = ("stream", "land", "up", "down", "across", "hidden", "result", "combine")
 
 
+def inner(n_z, z):
+    return int(0 < z < n_z - 1)
+
+
 def full_rows(n_z, source, target, half, q):
-    return abs(source - target) == 1 and half * 2 + q in FULL[0 < target < n_z - 1]
+    kind = inner(n_z, target) * (1 + inner(n_z, source))
+    return abs(source - target) == 1 and half * 2 + q in FULL[kind]
 
 
 def plan(n_z):
@@ -222,18 +228,18 @@
 
     def rank(z, event):
         kind, zq, h, half, q = event
-        away = abs(zq - z)
+        place = (inner(n_z, z) * 4 + abs(zq - z)) * 2 + half
         if kind in ("stream", "land"):
             return (RANK[0], 0.0, q)
         if kind == "combine":
-            return (RANK[1], COMB[away * 2 + half], q)
+            return (RANK[1], COMB[place], q)
         if kind == "result":
-            return (RANK[2], WORK[away * 2 + half], q)
+            return (RANK[2], WORK[place], q)
         if kind == "hidden":
-            return (RANK[3], WORK[away * 2 + half], q)
+            return (RANK[3], WORK[place], q)
         if kind == "across":
-            return (RANK[4], ROWX[away * 2 + half], q)
-        return (RANK[4], ROWZ[away * 2 + half] if h == 0 else ROWF[half], q)
+            return (RANK[4], ROWX[place], q)
+        return (RANK[4], ROWZ[place] if h == 0 else ROWF[inner(n_z, z) * 2 + half], q)
 
     order = {z: [] for z in zones}
     while any(todo.values()):
@@ -339,12 +345,12 @@
     halo_sem,
     sum_sem,
     fg_sem,
-    giv_send,
     giv_recv,
     z_send,
     x_send,
     c_send,
     b_recv,
+    s_recv,
     m_send,
     m_recv,
     hid_send,
@@ -379,6 +385,7 @@
     cols = res.shape[1]
     width = 2 * cols
     half_rows = tokens // SPLIT
+    n_chunks = 2 * SPLIT
     piece = half_rows // 2
     unit = wg.shape[2]
     pad = ext.shape[0] - tokens
@@ -400,36 +407,43 @@
             device_id_type=MESH,
         )
 
-    def chunk(zq, cq, h, half, q, ssem, dev):
-        ref = blk.at[zq * 2 + cq, h, half, pl.ds(q * piece, piece)]
-        return remote(ref, ref, ssem, b_recv.at[zq * 2 + cq, h, half, q], dev)
+    def chunk(zq, h, half, q, ssem, rsem, dev):
+        ref = blk.at[zq * 2 + c, half, h, pl.ds(q * piece, piece)]
+        return remote(ref, ref, ssem, rsem, dev)
 
     def side(h):
         return t + h * (1 - 2 * t)
 
     def z_copy(way, zq, h, half, q):
+        row = (zq + way) * (1 - h) + (n_z + 1 + way) * h
         return chunk(
-            zq, c, side(h), half, q, z_send.at[way, zq + h * (n_z - zq), half, q], targets[way]
+            zq,
+            side(h),
+            half,
+            q,
+            z_send.at[row, half, q],
+            b_recv.at[zq, side(h), half, q],
+            targets[way],
         )
 
     def x_copy(zq, half, q):
-        return chunk(zq, c, t, half, q, x_send.at[zq, half, q], peer)
+        return chunk(zq, t, half, q, x_send.at[zq, half, q], b_recv.at[zq, t, half, q], peer)
 
     def c_copy(zq, h, half, q):
-        return chunk(zq, c, h, half, q, c_send.at[zq, h, half, q], other)
-
-    def arrived(zq, cq, h, half, q):
-        chunk(zq, cq, h, half, q, c_send.at[zq, h, half, q], other).wait_recv()
+        return chunk(zq, h, half, q, c_send.at[zq, h, half, q], s_recv.at[zq, half], other)
+
+    def near_by(zq, half):
+        ref = blk.at[zq * 2 + 1 - c, half]
+        return remote(ref, ref, c_send.at[0, 0, 0, 0], s_recv.at[zq, half], other)
+
+    def arrived(zq, h, half, q):
+        chunk(zq, h, half, q, x_send.at[zq, half, q], b_recv.at[zq, h, half, q], peer).wait_recv()
 
     def m_copy(way, zq, cq, half):
         ref = meta.at[zq * 2 + cq, half]
-        return remote(
-            ref,
-            ref,
-            m_send.at[way, zq, half],
-            m_recv.at[zq * 2 + cq, half],
-            (up, down, other)[way],
-        )
+        row = zq + (0, 1, n_z + 1)[way]
+        ssem = m_send.at[row, half]
+        return remote(ref, ref, ssem, m_recv.at[zq * 2 + cq, half], (up, down, other)[way])
 
     def hid_copy(zq, half):
         return remote(
@@ -468,13 +482,13 @@
         return remote(hsend, hrecv, halo_sem.at[0], halo_sem.at[1], after)
 
     def sum_copy(r):
-        return remote(srow.at[0, r], srow.at[1, r], sum_sem.at[0, r], sum_sem.at[1, r], peer)
+        return remote(srow.at[0, r], srow.at[1, r], sum_sem.at[n_chunks + r], sum_sem.at[r], peer)
 
     def fg_copy():
         return remote(fg.at[t], fg.at[t], fg_sem.at[0], fg_sem.at[1], peer)
 
     def giv_copy(r):
-        return remote(gsend.at[r], grecv.at[r], giv_send.at[r], giv_recv.at[r], peer)
+        return remote(gsend.at[r], grecv.at[r], giv_recv.at[n_chunks + r], giv_recv.at[r], peer)
 
     barrier = pltpu.get_barrier_semaphore()
     cross_up = hi & (c == 1)
@@ -508,7 +522,7 @@
 
     docs = docs_ref[...].astype(F32)
     for k in range(tokens // lanes):
-        column = upright(docs[:, k * lanes : (k + 1) * lanes])
+        column = upright(docs[k : k + 1, :])
         dext[pad + k * lanes : pad + (k + 1) * lanes, :] = jnp.broadcast_to(column, (lanes, lanes))
     end_rows = product(pl.ds(tokens - tail, tail))
     hsend[:, :chan] = end_rows[tail - 8 :]
@@ -557,7 +571,6 @@
             ssq[rows, :] = jnp.broadcast_to(total, (step_rows, lanes))
             act[rows, :] = (conv_out * mix_ref[...]).astype(BF16)
 
-    n_chunks = 2 * SPLIT
     eye_piece = lax.broadcasted_iota(jnp.int32, (piece, lanes), 0) == lax.broadcasted_iota(
         jnp.int32, (piece, lanes), 1
     )
@@ -649,7 +662,7 @@
         for p, cq in sides():
             chosen, _ = picks(zq, cq, half)
             sel = jnp.concatenate(chosen, axis=0).astype(BF16)
-            got = normal_of([mm(sel, blk[zq * 2 + cq, h, half]) for h in range(2)])
+            got = normal_of([mm(sel, blk[zq * 2 + cq, half, h]) for h in range(2)])
             for h in range(2):
                 for e in range(EXP_DEV):
                     xs[e, p * most : (p + 1) * most, h * cols : (h + 1) * cols] = got[h][
@@ -659,7 +672,7 @@
             hid[t, zq, half, e] = silu_mul(mm(xs[e], wg[e]), mm(xs[e], wu[e]))
 
     def shared(half):
-        whole = normal_of([blk[z * 2 + c, h, half].astype(F32) for h in range(2)])
+        whole = normal_of([blk[z * 2 + c, half, h].astype(F32) for h in range(2)])
         gate = mm(whole[0], sg[:cols, :]) + mm(whole[1], sg[cols:, :])
         upper = mm(whole[0], su[:cols, :]) + mm(whole[1], su[cols:, :])
         shid[t, half] = silu_mul(gate, upper)
@@ -704,7 +717,7 @@
         scale = lax.rsqrt((ssq[rows, 0:1] + theirs) / (2 * chan) + 1e-06)
         giv_copy(r).wait_recv()
         proj = (kept + grecv[r].astype(F32)) * scale
-        blk[z * 2 + c, t, half, strip(q), :] = (res[rows, :].astype(F32) + proj).astype(BF16)
+        blk[z * 2 + c, half, t, strip(q), :] = (res[rows, :].astype(F32) + proj).astype(BF16)
         c_copy(z, t, half, q).start()
 
         @pl.when(r == GIVEN[0])
@@ -723,7 +736,7 @@
             m_copy(2, zq, c, half).wait_recv()
             m_copy(2, zq, c, half).start()
 
-        arrived(zq, c, side(h), half, q)
+        arrived(zq, side(h), half, q)
         c_copy(zq, side(h), half, q).start()
 
     def on_z(way):
@@ -741,9 +754,7 @@
 
     def on_hidden(zq, h, half, q):
         m_copy(2, zq, 1 - c, half).wait_recv()
-        for hh in range(2):
-            for qq in range(2):
-                arrived(zq, 1 - c, hh, half, qq)
+        near_by(zq, half).wait_recv()
         hidden(zq, half)
         hid_copy(zq, half).start()
 
@@ -770,7 +781,7 @@
             sh_copy(half).wait_recv()
 
         fin = (
-            blk[z * 2 + c, t, half, rows, :].astype(F32)
+            blk[z * 2 + c, half, t, rows, :].astype(F32)
             + mm(shid[0, half, rows, :], sd[:unit, :])
             + mm(shid[1, half, rows, :], sd[unit:, :])
             + acc[z, half, rows, :].astype(F32)
@@ -838,16 +849,13 @@
         on_combine,
     )
     order, _ = plan(n_z)
-    groups = max(-(-len(order[zz]) // 3) for zz in range(n_z))
-    tables = [encode(order[zz], 3 * groups) for zz in range(n_z)]
-    values = [
-        sum((z == zz).astype(jnp.int32) * tables[zz][g] for zz in range(n_z)) for g in range(groups)
-    ]
-
-    @pl.loop(0, groups)
-    def _(g):
-        value = sum((g == k).astype(jnp.int32) * values[k] for k in range(groups))
-
+    groups = [-(-len(order[zz]) // 3) for zz in range(n_z)]
+    tables = [encode(order[zz], 3 * max(groups)) for zz in range(n_z)]
+
+    def of_zone(numbers):
+        return sum((z == zz).astype(jnp.int32) * numbers[zz] for zz in range(n_z))
+
+    def act_on(value):
         def turn(k, rest):
             mark = rest % BASE + 31
             q, half, h = mark % 2, mark // 2 % 2, mark // 4 % 2
@@ -861,6 +869,25 @@
 
         lax.fori_loop(0, 3, turn, value)
 
+    span = 8
+    values = [of_zone([table[g] for table in tables]) for g in range(max(groups))]
+    values += [jnp.int32(0)] * (-len(values) % span)
+
+    def among(k, options):
+        return sum((k == n).astype(jnp.int32) * option for n, option in enumerate(options))
+
+    count = of_zone(groups)
+
+    @pl.loop(0, len(values) // span)
+    def _(page):
+        lines = [among(page, values[n::span]) for n in range(span)]
+
+        def line(n, carry):
+            act_on(among(n, lines))
+            return carry
+
+        lax.fori_loop(0, jnp.clip(count - page * span, 0, span), line, 0)
+
     @pl.when(has_next)
     def _():
         halo_copy().wait_send()
@@ -876,16 +903,20 @@
         for q in range(2):
             out_copy(half, q).wait()
 
-    def listed(target, half, q):
-        inner = (target > 0) & (target < n_z - 1)
-        outer_in, inner_in = half * 2 + q in FULL[0], half * 2 + q in FULL[1]
-        return (inner & inner_in) | (jnp.logical_not(inner) & outer_in)
+    def listed(source, target, half, q):
+        inside = [(one > 0) & (one < n_z - 1) for one in (source, target)]
+        to_end, from_end, both = [half * 2 + q in kind for kind in FULL]
+        return (
+            (jnp.logical_not(inside[1]) & to_end)
+            | (inside[1] & jnp.logical_not(inside[0]) & from_end)
+            | (inside[1] & inside[0] & both)
+        )
 
     for half in range(SPLIT):
         for q in range(2):
             for way, there, target in ((0, hi, z + 1), (1, lo, z - 1)):
 
-                @pl.when(there & listed(target, half, q))
+                @pl.when(there & listed(z, target, half, q))
                 def _():
                     z_copy(way, z, 1, half, q).wait_send()
 
@@ -903,21 +934,19 @@
         near = (zq == z + 1) | (zq == z - 1)
         for half in range(SPLIT):
             m_copy(2, zq, c, half).wait_send()
+            hid_copy(zq, half).wait_send()
             for q in range(2):
-
-                @pl.when(jnp.logical_not(near & listed(z, half, q)))
-                def _():
-                    x_copy(zq, half, q).wait_send()
-
+                sib_copy(zq, half, q).wait_send()
                 for h in range(2):
                     c_copy(zq, h, half, q).wait_send()
-                sib_copy(zq, half, q).wait_send()
 
                 @pl.when(zq != z)
                 def _():
                     back_copy(zq, half, q, zq, up).wait_send()
 
-            hid_copy(zq, half).wait_send()
+                @pl.when(jnp.logical_not(near & listed(zq, z, half, q)))
+                def _():
+                    x_copy(zq, half, q).wait_send()
 
 
 def fast(
@@ -981,7 +1010,7 @@
             pltpu.VMEM((2 * SPLIT, piece, cols), BF16),
             pltpu.VMEM((2, 1, cols), F32),
             pltpu.VMEM((rows, rows), BF16),
-            pltpu.VMEM((blocks, 2, SPLIT, rows, cols), BF16),
+            pltpu.VMEM((blocks, SPLIT, 2, rows, cols), BF16),
             pltpu.VMEM((blocks, SPLIT, 8, rows + -rows % lanes), F32),
             pltpu.VMEM((EXP_DEV, 2 * most, width), BF16),
             pltpu.VMEM((2, n_z, SPLIT, EXP_DEV, 2 * most, unit), BF16),
@@ -994,15 +1023,15 @@
             pltpu.VMEM((SPLIT, rows, cols), BF16),
             dma((11,)),
             dma((2,)),
-            dma((2, 2 * SPLIT)),
+            dma((4 * SPLIT,)),
             dma((2,)),
-            dma((2 * SPLIT,)),
-            dma((2 * SPLIT,)),
-            dma((2, n_z + 1, SPLIT, 2)),
+            dma((4 * SPLIT,)),
+            dma((n_z + 3, SPLIT, 2)),
             dma((n_z, SPLIT, 2)),
             dma((n_z, 2, SPLIT, 2)),
-            dma((blocks, 2, SPLIT, 2)),
-            dma((3, n_z, SPLIT)),
+            dma((n_z, 2, SPLIT, 2)),
+            dma((n_z, SPLIT)),
+            dma((2 * n_z + 1, SPLIT)),
             dma((blocks, SPLIT)),
             dma((n_z, SPLIT)),
             dma((n_z, SPLIT)),
@@ -1023,7 +1052,7 @@
         conv_input,
         residual,
         out_weight,
-        doc_ids[None, :],
+        doc_ids.reshape(tokens // lanes, lanes),
         conv_taps,
         mix_gain[None, :],
         ffn_gain[None, :],

time: 120 us -> 115 us (0.958)
  Pallas kernels: 116 us -> 113 us
  local copies, waits for them, and re-layouts: 3.31 us -> 2.06 us
    pallas_call x1, Pallas kernels: 116 us -> 113 us  [fast(): pl.pallas_call(functools.partial(layer_kernel, n_z, most), out_shape=jax....]
    broadcast_in_dim x1 -> x0, local copies, waits for them, and re-layouts: 1.24 us -> none  [fast(): doc_ids[None, :]]
where the time goes in v4:
time: 115 us
  Pallas kernels  113 us (98%)
  local copies, waits for them, and re-layouts  2.06 us (2%)
    pallas_call x1, Pallas kernels, fast(): pl.pallas_call(functools.partial(layer_kernel, n_z, most), out_shape=jax....  113 us

profile of v4, /device:TPU:0, one launch (start us, length us, event | category | flops | bytes accessed | tf_op | source)
XLA Modules:
  0.0 114.9 jit_solution(3166331641029709162)
XLA Ops:
  0.0 112.8 %shard_map.163 = bf16[384,1024]{1,0:T(8,128)(2,1)} custom-call(bf16[384,512]{1,0:T(8,128)(2,1)} %og_hbm.1, bf16[384,512]{1,0:T(8,128)(2,1)} %ig_hbm.1, bf16[384,512]{1,0:T(8,128)(2,1)} %ci_hbm.1, bf16[384,1024]{1,0:T(8,128)(2,1)} %res_hbm.1, bf16[512,2048]{1,0:T(8,128)(2,1)} %wo_hbm.1, s32[3,128]{1,0:T(4,128)} %bitcast.8, f32[3,512]{1,0:T(4,128)} %taps_ref.1, ...), custom_call_target="tpu_custom_call" | custom-call | tf_op jit(solution)/shard_map/pallas_call | solution.py:985
  112.8 2.1 %copy.19 = bf16[384,1024]{1,0:T(8,128)(2,1)} copy(bf16[384,1024]{1,0:T(8,128)(2,1)} %shard_map.163) | data formatting | bytes 1572864

commit v5 on v4

--- a/solution.py
+++ b/solution.py
@@ -415,41 +415,48 @@
         return t + h * (1 - 2 * t)
 
     def z_copy(way, zq, h, half, q):
-        row = (zq + way) * (1 - h) + (n_z + 1 + way) * h
+        ssem = z_send.at[way, zq + h * (n_z - zq + half * 2 + q)]
         return chunk(
-            zq,
-            side(h),
-            half,
-            q,
-            z_send.at[row, half, q],
-            b_recv.at[zq, side(h), half, q],
-            targets[way],
+            zq, side(h), half, q, ssem, b_recv.at[zq, side(h), half, q], targets[way]
         )
+
+    def z_sent(way, zq):
+        ref = blk.at[0]
+        return remote(ref.at[0], ref.at[0], z_send.at[way, zq], b_recv.at[0, 0, 0, 0], targets[way])
 
     def x_copy(zq, half, q):
         return chunk(zq, t, half, q, x_send.at[zq, half, q], b_recv.at[zq, t, half, q], peer)
 
     def c_copy(zq, h, half, q):
-        return chunk(zq, h, half, q, c_send.at[zq, h, half, q], s_recv.at[zq, half], other)
+        return chunk(zq, h, half, q, c_send.at[0], s_recv.at[zq, half], other)
+
+    def c_all():
+        ref = blk.at[pl.ds(0, n_z)]
+        return remote(ref, ref, c_send.at[0], s_recv.at[0, 0], other)
 
     def near_by(zq, half):
         ref = blk.at[zq * 2 + 1 - c, half]
-        return remote(ref, ref, c_send.at[0, 0, 0, 0], s_recv.at[zq, half], other)
+        return remote(ref, ref, c_send.at[0], s_recv.at[zq, half], other)
 
     def arrived(zq, h, half, q):
-        chunk(zq, h, half, q, x_send.at[zq, half, q], b_recv.at[zq, h, half, q], peer).wait_recv()
+        chunk(zq, h, half, q, c_send.at[0], b_recv.at[zq, h, half, q], other).wait_recv()
 
     def m_copy(way, zq, cq, half):
         ref = meta.at[zq * 2 + cq, half]
-        row = zq + (0, 1, n_z + 1)[way]
-        ssem = m_send.at[row, half]
+        ssem = m_send.at[way * n_z + zq * (way < 2)]
         return remote(ref, ref, ssem, m_recv.at[zq * 2 + cq, half], (up, down, other)[way])
+
+    def m_sent(way, zq):
+        ref = meta.at[0] if way < 2 else meta.at[pl.ds(0, n_z)]
+        return remote(
+            ref, ref, m_send.at[way * n_z + zq], m_recv.at[0, 0], (up, down, other)[way]
+        )
 
     def hid_copy(zq, half):
         return remote(
             hid.at[t, zq, half],
             hid.at[t, zq, half],
-            hid_send.at[zq, half],
+            hid_send.at[0],
             hid_recv.at[zq, half],
             peer,
         )
@@ -464,7 +471,7 @@
         return remote(
             outgo.at[zq, half, rows],
             sib.at[zq, half, rows],
-            sib_send.at[zq, half, q],
+            sib_send.at[0],
             sib_recv.at[zq, half, q],
             other,
         )
@@ -473,7 +480,7 @@
         return remote(
             acc.at[zq, half, pl.ds(q * piece, piece)],
             back.at[to, half, pl.ds(q * piece, piece)],
-            back_send.at[zq, half, q],
+            back_send.at[0],
             back_recv.at[to, half, q],
             dev,
         )
@@ -482,13 +489,13 @@
         return remote(hsend, hrecv, halo_sem.at[0], halo_sem.at[1], after)
 
     def sum_copy(r):
-        return remote(srow.at[0, r], srow.at[1, r], sum_sem.at[n_chunks + r], sum_sem.at[r], peer)
+        return remote(srow.at[0, r], srow.at[1, r], sum_sem.at[n_chunks], sum_sem.at[r], peer)
 
     def fg_copy():
         return remote(fg.at[t], fg.at[t], fg_sem.at[0], fg_sem.at[1], peer)
 
     def giv_copy(r):
-        return remote(gsend.at[r], grecv.at[r], giv_recv.at[n_chunks + r], giv_recv.at[r], peer)
+        return remote(gsend.at[r], grecv.at[r], giv_recv.at[n_chunks], giv_recv.at[r], peer)
 
     barrier = pltpu.get_barrier_semaphore()
     cross_up = hi & (c == 1)
@@ -893,11 +900,16 @@
         halo_copy().wait_send()
 
     fg_copy().wait_send()
-    for r in range(n_chunks):
-        sum_copy(r).wait_send()
-        giv_copy(r).wait_send()
+    remote(srow.at[0], srow.at[0], sum_sem.at[n_chunks], sum_sem.at[0], peer).wait_send()
+    remote(gsend, gsend, giv_recv.at[n_chunks], giv_recv.at[0], peer).wait_send()
     for half in range(SPLIT):
         sh_copy(half).wait_send()
+    c_all().wait_send()
+    m_sent(2, 0).wait_send()
+    remote(hid.at[t], hid.at[t], hid_send.at[0], hid_recv.at[0, 0], peer).wait_send()
+    remote(outgo, outgo, sib_send.at[0], sib_recv.at[0, 0, 0], other).wait_send()
+    sent = acc.at[pl.ds(0, n_z - 1)]
+    remote(sent, sent, back_send.at[0], back_recv.at[0, 0, 0], up).wait_send()
 
     for half in range(SPLIT):
         for q in range(2):
@@ -926,23 +938,12 @@
 
             @pl.when(there)
             def _():
-                for half in range(SPLIT):
-                    m_copy(way, zq, c, half).wait_send()
-                    for q in range(2):
-                        z_copy(way, zq, 0, half, q).wait_send()
+                m_sent(way, zq).wait_send()
+                z_sent(way, zq).wait_send()
 
         near = (zq == z + 1) | (zq == z - 1)
         for half in range(SPLIT):
-            m_copy(2, zq, c, half).wait_send()
-            hid_copy(zq, half).wait_send()
             for q in range(2):
-                sib_copy(zq, half, q).wait_send()
-                for h in range(2):
-                    c_copy(zq, h, half, q).wait_send()
-
-                @pl.when(zq != z)
-                def _():
-                    back_copy(zq, half, q, zq, up).wait_send()
 
                 @pl.when(jnp.logical_not(near & listed(zq, z, half, q)))
                 def _():
@@ -1023,23 +1024,23 @@
             pltpu.VMEM((SPLIT, rows, cols), BF16),
             dma((11,)),
             dma((2,)),
-            dma((4 * SPLIT,)),
+            dma((2 * SPLIT + 1,)),
             dma((2,)),
-            dma((4 * SPLIT,)),
-            dma((n_z + 3, SPLIT, 2)),
+            dma((2 * SPLIT + 1,)),
+            dma((2, n_z + 2 * SPLIT)),
             dma((n_z, SPLIT, 2)),
-            dma((n_z, 2, SPLIT, 2)),
+            dma((1,)),
             dma((n_z, 2, SPLIT, 2)),
             dma((n_z, SPLIT)),
-            dma((2 * n_z + 1, SPLIT)),
+            dma((2 * n_z + 1,)),
             dma((blocks, SPLIT)),
-            dma((n_z, SPLIT)),
+            dma((1,)),
             dma((n_z, SPLIT)),
             dma((SPLIT,)),
             dma((SPLIT,)),
+            dma((1,)),
             dma((n_z, SPLIT, 2)),
-            dma((n_z, SPLIT, 2)),
-            dma((n_z, SPLIT, 2)),
+            dma((1,)),
             dma((n_z + 1, SPLIT, 2)),
             dma((SPLIT, 2)),
         ],

time: 115 us -> 114 us (level)
  no operation moved by 1% of the time
where the time goes in v5:
time: 114 us
  Pallas kernels  112 us (98%)
  local copies, waits for them, and re-layouts  2.06 us (2%)
    pallas_call x1, Pallas kernels, fast(): pl.pallas_call(functools.partial(layer_kernel, n_z, most), out_shape=jax....  112 us

profile of v5, /device:TPU:0, one launch (start us, length us, event | category | flops | bytes accessed | tf_op | source)
XLA Modules:
  0.0 113.8 jit_solution(5672649276348990084)
XLA Ops:
  0.0 111.7 %shard_map.163 = bf16[384,1024]{1,0:T(8,128)(2,1)} custom-call(bf16[384,512]{1,0:T(8,128)(2,1)} %og_hbm.1, bf16[384,512]{1,0:T(8,128)(2,1)} %ig_hbm.1, bf16[384,512]{1,0:T(8,128)(2,1)} %ci_hbm.1, bf16[384,1024]{1,0:T(8,128)(2,1)} %res_hbm.1, bf16[512,2048]{1,0:T(8,128)(2,1)} %wo_hbm.1, s32[3,128]{1,0:T(4,128)} %bitcast.8, f32[3,512]{1,0:T(4,128)} %taps_ref.1, ...), custom_call_target="tpu_custom_call" | custom-call | tf_op jit(solution)/shard_map/pallas_call | solution.py:986
  111.7 2.1 %copy.19 = bf16[384,1024]{1,0:T(8,128)(2,1)} copy(bf16[384,1024]{1,0:T(8,128)(2,1)} %shard_map.163) | data formatting | bytes 1572864

commit v6 on v5

--- a/solution.py
+++ b/solution.py
@@ -139,16 +139,16 @@
 
 
 GIVEN = (1, 0, 2, 3)
-HOP, START, WIRE, NEAR = 2.8, 4.5, 4.18, (1.4, 2.5)
-COST, EXTRA = (0.45, 0.15, 0.15, 0.15, 0.15, 1.65, 1.3, 0.22), (0.9, 0.3)
-FULL = ((0, 2, 3), (0,), (1, 2, 3))
-ROWX = (3.2, 7.8, -0.1, 7, 2.4, 1.9, -0.8, -4.5, -6.9, -1.3, -4.6, -1.2, -3.6, -2.7, -3.5, -1.3)
-ROWZ = (5.3, -4.7, 3.6, 4.1, 6.5, 4, 5.6, -2.5, -3.8, 5.1, 3.9, -2.9, -5.3, 4.7, -3.6, 0.2)
-ROWF = (-0.1, -5.8, 4.7, 4.9)
-COMB = (5, -4.9, -3.1, 0.6, -2, -2.4, 5.5, -0.2, -1.5, -3.6, -4.8, 1.4, -0.4, 7.5, -2.3, -2.3)
-WORK = (-3.4, 3.1, -3.1, 1.5, 1.1, -1.8, 5.4, -5.7, -0.1, 1.1, -4, 2.1, -4.3, 1.7, -0.5, 1)
-RANK = (4, 0, 0, 0, 4)
-DEPTH = (1, 2)
+HOP, START, WIRE, NEAR = 2.8, 4.0, 4.18, (1.4, 2.5)
+COST, EXTRA = (0.45, 0.15, 0.15, 0.15, 0.15, 1.65, 1.3, 0.2), (0.9, 0.15)
+FULL = ((1, 2, 3), (0,), (1, 2, 3))
+ROWX = (2.8, 4.5, -2, 6, -4.8, 0.1, 0.2, -4.4, -7.7, 3.3, -10, 3.7, -0.2, 0.7, 5.9, -0.4)
+ROWZ = (0.5, -2.7, 0.5, -2.4, -4.1, -0.1, 2.8, -6.3, 4.6, 2.6, 2.3, 1.4, 0.3, -0.9, -3, 4.4)
+ROWF = (1.3, 3, -5.7, 3.9)
+COMB = (1.7, 3.6, 3.6, -1.7, 5.9, 5.1, -0.3, -0.2, -6, -1.4, -3.2, -5.6, -1, 1.9, 2, 3.1)
+WORK = (6.6, -4.2, -3.5, 5.1, 1.1, 4.1, -1.4, 2.4, -4.3, 4.5, 1.2, -5.4, 2.4, -4.2, -3.7, 5.7)
+RANK = (3, 4, 3, 4, 4)
+DEPTH = (0.5, 2)
 BASE = 257
 
 
@@ -168,7 +168,7 @@
     chunks = [(half, q) for half in range(SPLIT) for q in range(2)]
     zones = range(n_z)
     never = 1e9
-    have, told, heard, summed, went, final, arrive = {}, {}, {}, {}, {}, {}, {}
+    have, told, heard, summed, went, begun, final, arrive = {}, {}, {}, {}, {}, {}, {}, {}
     todo = {z: [] for z in zones}
     for z in zones:
         for k, (half, q) in enumerate(chunks):
@@ -185,7 +185,7 @@
                     todo[z].append(("down", zq, 0, half, q))
                 if not full_rows(n_z, zq, z, half, q):
                     todo[z].append(("across", zq, 0, half, q))
-                todo[z].append(("combine", zq, 0, half, q))
+                todo[z] += [("combine", zq, h, half, q) for h in range(2)]
             for half in range(SPLIT):
                 todo[z].append(("hidden", zq, 0, half, 0))
                 todo[z].append(("result", zq, 0, half, 0))
@@ -219,11 +219,13 @@
             return heard.get((z, zq, half), never)
         at = told.get((z, zq, half), never)
         if zq >= z and z > 0:
-            at = max(at, summed.get((z - 1, zq, half, q), never))
+            at = max(at, summed.get((z - 1, zq, h, half, q), never))
         if zq <= z and z < n_z - 1:
-            at = max(at, summed.get((z + 1, zq, half, q), never))
+            at = max(at, summed.get((z + 1, zq, h, half, q), never))
+        if h > 0:
+            at = max(at, begun.get((z, zq, half, q), never))
         if zq == z and q > 0:
-            at = max(at, final.get((z, half, q - 1), never))
+            at = max(at, begun.get((z, zq, half, 0), never))
         return at
 
     def rank(z, event):
@@ -271,10 +273,13 @@
             heard[z, zq, half] = put(z, "across", end, 1.0 if zq == z else 0.5)
         elif kind == "result":
             told[z, zq, half] = end + NEAR[1]
-        elif zq == z:
-            final[z, half, q] = end
         else:
-            summed[z, zq, half, q] = put(z, "up" if zq > z else "down", end, 1.0)
+            if h == 0:
+                begun[z, zq, half, q] = end
+            if zq == z:
+                final[z, h, half, q] = end
+            else:
+                summed[z, zq, h, half, q] = put(z, "up" if zq > z else "down", end, 0.5)
     return order, max(final.values())
 
 
@@ -387,6 +392,7 @@
     half_rows = tokens // SPLIT
     n_chunks = 2 * SPLIT
     piece = half_rows // 2
+    part_rows = piece // 2
     unit = wg.shape[2]
     pad = ext.shape[0] - tokens
     lo = z > 0
@@ -476,12 +482,13 @@
             other,
         )
 
-    def back_copy(zq, half, q, to, dev):
+    def back_copy(zq, half, p, to, dev):
+        rows = pl.ds(p * part_rows, part_rows)
         return remote(
-            acc.at[zq, half, pl.ds(q * piece, piece)],
-            back.at[to, half, pl.ds(q * piece, piece)],
+            acc.at[zq, half, rows],
+            back.at[to, half, rows],
             back_send.at[0],
-            back_recv.at[to, half, q],
+            back_recv.at[to, half, p],
             dev,
         )
 
@@ -598,13 +605,10 @@
         giv_copy(r).start()
 
     first[2].wait()
-    for r in GIVEN:
-        if r:
-            convolve(r)
-            sums(r)
+    convolve(GIVEN[0])
+    sums(GIVEN[0])
     first[3].wait()
     give(GIVEN[0])
-    first[4].wait()
     arrivals = (
         2
         + lo.astype(jnp.int32)
@@ -634,9 +638,10 @@
         ext[pad - 8 : pad, :] = jnp.zeros((8, chan), F32)
         dext[pad - 8 : pad, :] = jnp.zeros((8, lanes), F32)
 
-    convolve(0)
-    sums(0)
+    first[4].wait()
     for r in GIVEN[1:]:
+        convolve(r)
+        sums(r)
         give(r)
         send_given(r)
     fg_copy().wait_recv()
@@ -773,17 +778,15 @@
     def on_result(zq, h, half, q):
         results(zq, half)
 
-    def out_copy(half, q):
+    def out_copy(half, p):
         return pltpu.make_async_copy(
-            done.at[half, pl.ds(q * piece, piece)],
-            out_hbm.at[pl.ds(half * half_rows + q * piece, piece)],
-            out_sem.at[half, q],
+            done.at[half, pl.ds(p * part_rows, part_rows)],
+            out_hbm.at[pl.ds(half * half_rows + p * part_rows, part_rows)],
+            out_sem.at[half, p],
         )
 
-    def finish(half, q):
-        rows = strip(q)
-
-        @pl.when(q == 0)
+    def finish(half, p, rows):
+        @pl.when(p == 0)
         def _():
             sh_copy(half).wait_recv()
 
@@ -797,24 +800,28 @@
 
         @pl.when(lo)
         def _():
-            back_copy(z, half, q, z, up).wait_recv()
+            back_copy(z, half, p, z, up).wait_recv()
 
         @pl.when(hi)
         def _():
-            back_copy(z, half, q, n_z, up).wait_recv()
+            back_copy(z, half, p, n_z, up).wait_recv()
 
         low = jnp.where(lo, back[z, half, rows, :].astype(F32), F32(0.0))
         high = jnp.where(hi, back[n_z, half, rows, :].astype(F32), F32(0.0))
         done[half, rows, :] = (fin + low + high).astype(BF16)
-        out_copy(half, q).start()
+        out_copy(half, p).start()
 
     def on_combine(zq, h, half, q):
-        rows = strip(q)
-        sib_copy(zq, half, q).wait_recv()
+        p = q * 2 + h
+        rows = pl.ds(pl.multiple_of(p * part_rows, part_rows), part_rows)
+
+        @pl.when(h == 0)
+        def _():
+            sib_copy(zq, half, q).wait_recv()
 
         @pl.when(zq == z)
         def _():
-            finish(half, q)
+            finish(half, p, rows)
 
         @pl.when(zq != z)
         def _():
@@ -826,7 +833,7 @@
 
             @pl.when(jnp.logical_not(is_end(zq)))
             def _():
-                back_copy(zq, half, q, zq, up).wait_recv()
+                back_copy(zq, half, p, zq, up).wait_recv()
                 acc[zq, half, rows, :] = (
                     acc[zq, half, rows, :].astype(F32)
                     + sib[zq, half, rows, :].astype(F32)
@@ -835,15 +842,15 @@
 
             @pl.when(zq > z)
             def _():
-                back_copy(zq, half, q, zq, up).start()
+                back_copy(zq, half, p, zq, up).start()
 
             @pl.when(zq < z - 1)
             def _():
-                back_copy(zq, half, q, zq, down).start()
+                back_copy(zq, half, p, zq, down).start()
 
             @pl.when(zq == z - 1)
             def _():
-                back_copy(zq, half, q, n_z, down).start()
+                back_copy(zq, half, p, n_z, down).start()
 
     actions = (
         on_stream,
@@ -912,8 +919,8 @@
     remote(sent, sent, back_send.at[0], back_recv.at[0, 0, 0], up).wait_send()
 
     for half in range(SPLIT):
-        for q in range(2):
-            out_copy(half, q).wait()
+        for p in range(4):
+            out_copy(half, p).wait()
 
     def listed(source, target, half, q):
         inside = [(one > 0) & (one < n_z - 1) for one in (source, target)]
@@ -1041,8 +1048,8 @@
             dma((1,)),
             dma((n_z, SPLIT, 2)),
             dma((1,)),
-            dma((n_z + 1, SPLIT, 2)),
-            dma((SPLIT, 2)),
+            dma((n_z + 1, SPLIT, 4)),
+            dma((SPLIT, 4)),
         ],
         compiler_params=pltpu.CompilerParams(
             collective_id=0, has_side_effects=True, vmem_limit_bytes=64 * 1024 * 1024 - 65536

time: 114 us -> 114 us (level)
  no operation moved by 1% of the time
where the time goes in v6:
time: 114 us
  Pallas kernels  112 us (98%)
  local copies, waits for them, and re-layouts  2.06 us (2%)
    pallas_call x1, Pallas kernels, fast(): pl.pallas_call(functools.partial(layer_kernel, n_z, most), out_shape=jax....  112 us

profile of v6, /device:TPU:0, one launch (start us, length us, event | category | flops | bytes accessed | tf_op | source)
XLA Modules:
  0.0 113.7 jit_solution(2277896807042783357)
XLA Ops:
  0.0 111.7 %shard_map.163 = bf16[384,1024]{1,0:T(8,128)(2,1)} custom-call(bf16[384,512]{1,0:T(8,128)(2,1)} %og_hbm.1, bf16[384,512]{1,0:T(8,128)(2,1)} %ig_hbm.1, bf16[384,512]{1,0:T(8,128)(2,1)} %ci_hbm.1, bf16[384,1024]{1,0:T(8,128)(2,1)} %res_hbm.1, bf16[512,2048]{1,0:T(8,128)(2,1)} %wo_hbm.1, s32[3,128]{1,0:T(4,128)} %bitcast.8, f32[3,512]{1,0:T(4,128)} %taps_ref.1, ...), custom_call_target="tpu_custom_call" | custom-call | tf_op jit(solution)/shard_map/pallas_call | solution.py:993
  111.7 2.1 %copy.19 = bf16[384,1024]{1,0:T(8,128)(2,1)} copy(bf16[384,1024]{1,0:T(8,128)(2,1)} %shard_map.163) | data formatting | bytes 1572864

commit v7 on v6

--- a/solution.py
+++ b/solution.py
@@ -782,7 +782,7 @@
         return pltpu.make_async_copy(
             done.at[half, pl.ds(p * part_rows, part_rows)],
             out_hbm.at[pl.ds(half * half_rows + p * part_rows, part_rows)],
-            out_sem.at[half, p],
+            out_sem.at[0],
         )
 
     def finish(half, p, rows):
@@ -918,9 +918,7 @@
     sent = acc.at[pl.ds(0, n_z - 1)]
     remote(sent, sent, back_send.at[0], back_recv.at[0, 0, 0], up).wait_send()
 
-    for half in range(SPLIT):
-        for p in range(4):
-            out_copy(half, p).wait()
+    pltpu.make_async_copy(res, out_hbm, out_sem.at[0]).wait()
 
     def listed(source, target, half, q):
         inside = [(one > 0) & (one < n_z - 1) for one in (source, target)]
@@ -1049,7 +1047,7 @@
             dma((n_z, SPLIT, 2)),
             dma((1,)),
             dma((n_z + 1, SPLIT, 4)),
-            dma((SPLIT, 4)),
+            dma((1,)),
         ],
         compiler_params=pltpu.CompilerParams(
             collective_id=0, has_side_effects=True, vmem_limit_bytes=64 * 1024 * 1024 - 65536

time: 114 us -> 114 us (level)
  no operation moved by 1% of the time
where the time goes in v7:
time: 114 us
  Pallas kernels  112 us (98%)
  local copies, waits for them, and re-layouts  2.06 us (2%)
    pallas_call x1, Pallas kernels, fast(): pl.pallas_call(functools.partial(layer_kernel, n_z, most), out_shape=jax....  112 us

profile of v7, /device:TPU:0, one launch (start us, length us, event | category | flops | bytes accessed | tf_op | source)
XLA Modules:
  0.0 113.7 jit_solution(10002399191931178727)
XLA Ops:
  0.0 111.6 %shard_map.163 = bf16[384,1024]{1,0:T(8,128)(2,1)} custom-call(bf16[384,512]{1,0:T(8,128)(2,1)} %og_hbm.1, bf16[384,512]{1,0:T(8,128)(2,1)} %ig_hbm.1, bf16[384,512]{1,0:T(8,128)(2,1)} %ci_hbm.1, bf16[384,1024]{1,0:T(8,128)(2,1)} %res_hbm.1, bf16[512,2048]{1,0:T(8,128)(2,1)} %wo_hbm.1, s32[3,128]{1,0:T(4,128)} %bitcast.8, f32[3,512]{1,0:T(4,128)} %taps_ref.1, ...), custom_call_target="tpu_custom_call" | custom-call | tf_op jit(solution)/shard_map/pallas_call | solution.py:991
  111.6 2.1 %copy.19 = bf16[384,1024]{1,0:T(8,128)(2,1)} copy(bf16[384,1024]{1,0:T(8,128)(2,1)} %shard_map.163) | data formatting | bytes 1572864
